TPU v7x, 512 devices: a whole 4x8x8 slice. The times are simulated.
512 devices in a mesh: fs: 64 (over z, y), tp: 8 (over x, core).
Axes of the slice: x: 4, y: 8, z: 8, core: 2. Of those that a mesh axis runs over, the one named last changes fastest.
Arguments:
- tokens: bfloat16 [16384, 2048], P('fs', 'tp'), may hold values from -6 to 6
- mixer_norm_gain: bfloat16 [2048], replicated, may hold values from 0.099609375 to 1.8984375
- recurrence_branch_weight: bfloat16 [2048, 1024], P('fs', 'tp'), may hold values from -0.125 to 0.125
- output_gate_projection: bfloat16 [2048, 1024], P('fs', 'tp'), may hold values from -0.125 to 0.125
- recurrence_conv_taps: bfloat16 [4, 1024], P(None, 'tp'), may hold values from -3 to 3
- recurrence_gate_map: bfloat16 [16, 64, 64], P('tp'), may hold values from -0.75 to 0.75
- input_gate_map: bfloat16 [16, 64, 64], P('tp'), may hold values from -0.75 to 0.75
- channel_decay_rate: float32 [1024], P('tp'), may hold values from 0.001 to 0.03
- position_log_decay: float32 [16384, 1024], P('fs', 'tp'), may hold values from -0.69 to 0
- mixer_output_weight: bfloat16 [1024, 2048], P('tp', 'fs'), may hold values from -0.75 to 0.75
- feedforward_norm_gain: bfloat16 [2048], replicated, may hold values from 0.099609375 to 1.8984375
- gate_up_weight: bfloat16 [2048, 5632], P('fs', 'tp'), may hold values from -0.125 to 0.125
- value_up_weight: bfloat16 [2048, 5632], P('fs', 'tp'), may hold values from -0.125 to 0.125
- gate_conv_taps: bfloat16 [3, 5632], P(None, 'tp'), may hold values from -3 to 3
- value_conv_taps: bfloat16 [3, 5632], P(None, 'tp'), may hold values from -3 to 3
- down_projection_weight: bfloat16 [5632, 2048], P('tp', 'fs'), may hold values from -0.15625 to 0.15625
Outputs:
- result: bfloat16 [16384, 2048], P('fs', 'tp')
All inputs are finite; a program needn't handle non-finite values.
Results may differ from a plain program's by a relative error of at most 0.024.
Values may be sent and summed in bfloat16 or wider, within the bound.
A program may use at most 64 MiB of HBM per device.

v0:
```python
import jax
import jax.numpy as jnp
from jax import lax
from jax.sharding import Mesh
from jax.sharding import PartitionSpec as P

SEQ_LEN = 64
FS = ("fs_0", "fs_1")


EPS = 1e-06
DECAY_RATE_GAIN = 8.0


def in_order(parts, dim):
    lengths = list(parts.shape[1:])
    lengths[dim] *= parts.shape[0]
    return jnp.moveaxis(parts, 0, dim).reshape(lengths)


def from_everyone(array, axis):
    size = lax.axis_size(axis)
    return lax.all_to_all(
        jnp.broadcast_to(array[None], (size, *array.shape)), axis, 0, 0, tiled=True
    )


def gather_directly(array, axis, dim):
    return in_order(from_everyone(array, axis), dim)


def side_by_side(arrays, axis, dim, along):
    widths = [a.shape[along] for a in arrays]
    both = jnp.concatenate(arrays, axis=along)
    result = lax.all_gather(both, axis, axis=dim, tiled=True)
    return tuple(jnp.split(result, [sum(widths[:k]) for k in range(1, len(widths))], axis=along))


def in_blocks(array, dim, size):
    before, after = (array.shape[:dim], array.shape[dim + 1 :])
    return jnp.moveaxis(array.reshape(*before, size, -1, *after), dim, 0)


def sent_and_summed(array, axis, dim):
    size = lax.axis_size(axis)
    parts = lax.all_to_all(in_blocks(array, dim, size), axis, 0, 0, tiled=True)
    return jnp.sum(parts.astype(jnp.float32), axis=0)


def all_blocks(array, axes, turns):
    parts = array
    for k in turns:
        parts = lax.all_gather(parts, axes[k])
    done = turns[::-1]
    back = [done.index(k) for k in range(len(axes))]
    parts = parts.transpose(*back, *range(len(axes), parts.ndim))
    return parts.reshape(-1, *array.shape)


def gather_axes(array, axes, turns, dim):
    return in_order(all_blocks(array, axes, turns), dim)


def rms_normed(values, gain):
    wide = values.astype(jnp.float32)
    factor = lax.rsqrt(jnp.mean(wide * wide, axis=-1, keepdims=True) + EPS)
    return (wide * factor * gain.astype(jnp.float32)).astype(jnp.bfloat16)


def causal_conv(values, kernel):
    width = kernel.shape[0]
    row_count, channels = values.shape
    grouped = values.astype(jnp.float32).reshape(row_count // SEQ_LEN, SEQ_LEN, channels)
    padded = jnp.pad(grouped, ((0, 0), (width - 1, 0), (0, 0)))
    summed = padded[:, 0:SEQ_LEN] * kernel[0].astype(jnp.float32)
    for offset in range(1, width):
        summed = summed + padded[:, offset : offset + SEQ_LEN] * kernel[offset].astype(jnp.float32)
    return summed.reshape(row_count, channels)


def combine(left, right):
    first_a, first_b = left
    second_a, second_b = right
    return (first_a * second_a, second_a * first_b + second_b)


def pair_folder(normed, pieces):
    return (
        jnp.dot(normed, pieces[0], preferred_element_type=jnp.float32),
        jnp.dot(normed, pieces[1], preferred_element_type=jnp.float32),
    )


def per_device(
    tokens,
    mixer_norm_gain,
    recurrence_branch_weight,
    output_gate_projection,
    recurrence_conv_taps,
    recurrence_gate_map,
    input_gate_map,
    channel_decay_rate,
    position_log_decay,
    mixer_output_weight,
    feedforward_norm_gain,
    gate_up_weight,
    value_up_weight,
    gate_conv_taps,
    value_conv_taps,
    down_projection_weight,
):
    row_count = tokens.shape[0]
    local_width = recurrence_branch_weight.shape[1]
    local_heads = recurrence_gate_map.shape[0]
    head_size = recurrence_gate_map.shape[1]
    whole_rows = gather_directly(tokens, "tp", 1)
    normed = rms_normed(whole_rows, mixer_norm_gain)
    branch_sum, outgate_sum = pair_folder(
        normed, side_by_side((recurrence_branch_weight, output_gate_projection), FS, 0, 1)
    )
    branch = branch_sum.astype(jnp.bfloat16)
    outgate = outgate_sum.astype(jnp.bfloat16)
    conv = causal_conv(branch, recurrence_conv_taps).astype(jnp.bfloat16)
    grouped = conv.reshape(row_count, local_heads, head_size)
    recurrence_scan = jax.nn.sigmoid(
        jnp.einsum(
            "rhi,hij->rhj", grouped, recurrence_gate_map, preferred_element_type=jnp.float32
        ).reshape(row_count, local_width)
    )
    inner = jax.nn.sigmoid(
        jnp.einsum(
            "rhi,hij->rhj", grouped, input_gate_map, preferred_element_type=jnp.float32
        ).reshape(row_count, local_width)
    )
    log_alpha = (
        -DECAY_RATE_GAIN * recurrence_scan * channel_decay_rate[None, :] + position_log_decay
    )
    drive = jnp.sqrt(-jnp.expm1(2.0 * log_alpha)) * inner * conv.astype(jnp.float32)
    shape3 = (row_count // SEQ_LEN, SEQ_LEN, local_width)
    unused, state = lax.associative_scan(
        combine, (jnp.exp(log_alpha).reshape(shape3), drive.reshape(shape3)), axis=1
    )
    state = state.reshape(row_count, local_width)
    mixed = (state * jax.nn.gelu(outgate.astype(jnp.float32))).astype(jnp.bfloat16)
    mixer_terms = jnp.dot(
        mixed, gather_directly(mixer_output_weight, FS, 1), preferred_element_type=jnp.float32
    )
    mixer_terms = mixer_terms.astype(jnp.bfloat16).astype(jnp.float32)
    mixer_share = sent_and_summed(mixer_terms.astype(jnp.bfloat16), "tp", 1)
    after_share = (tokens.astype(jnp.float32) + mixer_share).astype(jnp.bfloat16)
    whole_after = gather_directly(after_share, "tp", 1)
    normed2 = rms_normed(whole_after, feedforward_norm_gain)
    gate_whole, value_whole = side_by_side((gate_up_weight, value_up_weight), FS, 0, 1)
    gate_sum = jnp.dot(normed2, gate_whole, preferred_element_type=jnp.float32)
    value_sum = jnp.dot(normed2, value_whole, preferred_element_type=jnp.float32)
    gate_half = gate_sum.astype(jnp.bfloat16)
    value_half = value_sum.astype(jnp.bfloat16)
    hidden = (
        jax.nn.silu(causal_conv(gate_half, gate_conv_taps))
        * causal_conv(value_half, value_conv_taps)
    ).astype(jnp.bfloat16)
    channel_terms = jnp.dot(
        hidden,
        gather_axes(down_projection_weight, FS, (0, 1), 1),
        preferred_element_type=jnp.float32,
    )
    channel_terms = channel_terms.astype(jnp.bfloat16).astype(jnp.float32)
    channel_share = sent_and_summed(channel_terms.astype(jnp.bfloat16), "tp", 1)
    share_width = channel_share.shape[1]
    residual_share = lax.dynamic_slice_in_dim(
        whole_after, lax.axis_index("tp") * share_width, share_width, 1
    )
    return (residual_share.astype(jnp.float32) + channel_share).astype(jnp.bfloat16)


def solution(mesh):
    torus = Mesh(mesh.devices.reshape(8, 8, mesh.shape["tp"]), ("fs_0", "fs_1", "tp"))
    return jax.shard_map(
        per_device,
        mesh=torus,
        in_specs=(
            P(FS, "tp"),
            P(),
            P(FS, "tp"),
            P(FS, "tp"),
            P(None, "tp"),
            P("tp", None, None),
            P("tp", None, None),
            P("tp"),
            P(FS, "tp"),
            P("tp", FS),
            P(),
            P(FS, "tp"),
            P(FS, "tp"),
            P(None, "tp"),
            P(None, "tp"),
            P("tp", FS),
        ),
        out_specs=P(FS, "tp"),
        check_vma=False,
    )
```

profile of v0, /device:TPU:1, one launch (start us, length us, event | category | flops | bytes accessed | tf_op | source)
XLA Modules:
  0.0 284.1 jit_solution(3254994639831585429)
XLA Ops:
  6.5 1.3 pad_maximum_fusion.3
  7.9 0.0 all-gather.7.cloned.1.call-update
  7.9 0.0 all-gather.11.cloned.1.call-start
  7.9 28.3 %all-gather.2 = bf16[8,704,32]{1,2,0:T(8,128)(2,1)} all-gather(bf16[1,704,32]{1,2,0:T(8,128)(2,1)} %bitcast.112), channel_id=2, replica_groups=mesh['fs_0'=8,'fs_1'=8,'tp'=8] {'fs_0'}, dimensions={0}, use_global_device_ids=true | all-gather | bytes 405504 | tf_op jit(solution)/shard_map/all_gather | solution.py:53
  36.2 0.0 copy-start.8
  36.2 0.0 copy-start.5
  36.2 0.0 all-gather.11.cloned.1.call-update
  36.3 0.0 all-gather.9.cloned.1.call-start
  36.3 1.5 pad_maximum_fusion
  37.9 0.0 all-gather.9.cloned.1.call-update
  37.9 1.0 copy.68
  38.9 1.1 broadcast_in_dim.6
  40.0 11.4 %all-to-all-start = ((bf16[8,256,256]{1,2,0:T(8,128)(2,1)}), bf16[8,256,256]{1,2,0:T(8,128)(2,1)S(1)}, u32[]{:S(2)}, u32[]{:S(2)}) async-start(bf16[8,256,256]{1,2,0:T(8,128)(2,1)} %broadcast_in_dim.6), calls=%async_computation | async-start | bytes 2097152 | tf_op jit(solution)/shard_map/all_to_all | solution.py:23
  51.3 0.0 copy-done.6
  51.4 14.9 %all-to-all-done = bf16[8,256,256]{1,2,0:T(8,128)(2,1)S(1)} async-done(((bf16[8,256,256]{1,2,0:T(8,128)(2,1)}), bf16[8,256,256]{1,2,0:T(8,128)(2,1)S(1)}, u32[]{:S(2)}, u32[]{:S(2)}) %all-to-all-start) | async-done | bytes 1048608 | tf_op jit(solution)/shard_map/all_to_all | solution.py:23
  66.3 0.8 broadcast_in_dim.7
  67.1 9.7 %all-to-all-start.1 = ((bf16[64,128,32]{1,2,0:T(8,128)(2,1)}), bf16[64,128,32]{1,2,0:T(8,128)(2,1)S(1)}, u32[]{:S(2)}, u32[]{:S(2)}) async-start(bf16[64,128,32]{1,2,0:T(8,128)(2,1)} %broadcast_in_dim.7), calls=%async_computation.1 | async-start | bytes 1048576 | tf_op jit(solution)/shard_map/all_to_all | solution.py:23
  76.8 0.3 multiply_reduce_fusion.1
  77.2 0.3 fusion.5
  77.5 0.0 copy-start.9
  77.5 0.0 copy-start.2
  77.5 21.2 %all-gather.7.cloned.1.call-done = bf16[2048,256]{1,0:T(8,128)(2,1)} async-done(((bf16[32,256]{1,0:T(8,128)(2,1)}), bf16[2048,256]{1,0:T(8,128)(2,1)}) %all-gather.7.cloned.1.call-update) | async-done | bytes 1048592 | tf_op jit(solution)/shard_map/all_gather | solution.py:35
  98.7 1.5 convolution_convert_fusion.3
  100.3 0.1 fusion.41
  100.4 0.1 convert_element_type.222
  100.5 0.1 copy.69
  100.6 0.2 fusion.21
  100.8 0.1 copy.71
  100.9 0.0 copy-done.9
  100.9 0.2 fusion.23
  101.2 0.1 copy.74
  101.3 0.1 fusion.66
  102.0 0.1 pad.52
  102.1 0.1 pad.51
  102.9 0.0 all-to-all-done.1
  102.9 1.9 convolution_convert_fusion
  104.8 0.1 copy.90
  104.8 0.0 copy-start.1
  104.8 24.1 %all_to_all.25 = bf16[8,256,256]{2,1,0:T(8,128)(2,1)S(1)} all-to-all(bf16[8,256,256]{2,1,0:T(8,128)(2,1)S(1)} %bitcast.90), channel_id=1, replica_groups=mesh['fs_0'=8,'fs_1'=8,'tp'=8] {'tp'}, dimensions={0} | all-to-all | bytes 2097152 | tf_op jit(solution)/shard_map/all_to_all | solution.py:46
  128.9 0.1 convert_reduce_fusion.1
  129.1 0.0 copy-start.7
  129.1 0.0 copy-start.3
  129.1 0.0 copy-start.4
  129.2 1.1 broadcast_in_dim.8
  130.2 4.4 %all-to-all-start.3 = ((bf16[8,256,256]{2,1,0:T(8,128)(2,1)}), bf16[8,256,256]{2,1,0:T(8,128)(2,1)S(1)}, u32[]{:S(2)}, u32[]{:S(2)}) async-start(bf16[8,256,256]{2,1,0:T(8,128)(2,1)} %broadcast_in_dim.8), calls=%async_computation.3 | async-start | bytes 2097152 | tf_op jit(solution)/shard_map/all_to_all | solution.py:23
  134.7 0.1 convert_reduce_fusion.4
  134.8 14.9 %all-to-all-done.3 = bf16[8,256,256]{2,1,0:T(8,128)(2,1)S(1)} async-done(((bf16[8,256,256]{2,1,0:T(8,128)(2,1)}), bf16[8,256,256]{2,1,0:T(8,128)(2,1)S(1)}, u32[]{:S(2)}, u32[]{:S(2)}) %all-to-all-start.3) | async-done | bytes 1048608 | tf_op jit(solution)/shard_map/all_to_all | solution.py:23
  149.7 0.5 copy.76
  150.2 0.3 multiply_reduce_fusion
  150.5 0.2 all-gather.11.cloned.1.call-done
  150.7 3.8 %copy.80 = bf16[8,8,704,32]{2,3,1,0:T(8,128)(2,1)} copy(bf16[8,8,704,32]{2,3,0,1:T(8,128)(2,1)} %bitcast.91) | data formatting | bytes 5767168 | tf_op jit(solution)/shard_map/transpose | solution.py:56
  154.5 85.5 %all-gather.9.cloned.1.call-done = bf16[2048,1408]{1,0:T(8,128)(2,1)} async-done(((bf16[32,1408]{1,0:T(8,128)(2,1)}), bf16[2048,1408]{1,0:T(8,128)(2,1)}) %all-gather.9.cloned.1.call-update) | async-done | bytes 5767184 | tf_op jit(solution)/shard_map/all_gather | solution.py:35
  240.0 3.5 %fusion.9 = f32[256,704]{0,1:T(8,128)S(1)} fusion(bf16[2048,1408]{1,0:T(8,128)(2,1)} %all-gather.9.cloned.1.call-done, bf16[256,2048]{0,1:T(8,128)(2,1)S(1)} %bitcast.86, f32[2048]{0:T(1024)S(1)} %convert_element_type.234, f32[256]{0:T(256)S(1)} %add_rsqrt_fusion), kind=kOutput, calls=%fused_computation.15 | convolution fusion | flops 740655104 | bytes 4924416 | tf_op jit(solution)/shard_map/dot_general | solution.py:154
  243.5 0.3 copy.78
  243.7 4.9 %fusion.15 = f32[256,704]{0,1:T(8,128)S(1)} fusion(bf16[2048,1408]{1,0:T(8,128)(2,1)} %all-gather.9.cloned.1.call-done, bf16[256,2048]{0,1:T(8,128)(2,1)S(1)} %bitcast.87, f32[2048]{0:T(1024)S(1)} %convert_element_type.234, f32[256]{0:T(256)S(1)} %add_rsqrt_fusion), kind=kOutput, calls=%fused_computation.17 | convolution fusion | flops 740655104 | bytes 4924416 | tf_op jit(solution)/shard_map/dot_general | solution.py:155
  248.6 0.3 copy.79
  248.9 0.6 fusion.33
  249.5 2.9 %convolution_convert_fusion.1 = bf16[256,2048]{1,0:T(8,128)(2,1)S(1)} fusion(bf16[256,704]{1,0:T(8,128)(2,1)S(1)} %bitcast.105, bf16[704,2048]{0,1:T(8,128)(2,1)} %bitcast.92), kind=kOutput, calls=%fused_computation.5 | convolution fusion | flops 738721792 | bytes 4292608 | tf_op jit(solution)/shard_map/dot_general | solution.py:162
  252.4 1.0 copy.89
  253.5 8.3 %all-to-all-start.4 = ((bf16[8,256,256]{2,1,0:T(8,128)(2,1)}), bf16[8,256,256]{2,1,0:T(8,128)(2,1)S(1)}, u32[]{:S(2)}, u32[]{:S(2)}) async-start(bf16[8,256,256]{2,1,0:T(8,128)(2,1)} %bitcast.73), calls=%async_computation.4 | async-start | bytes 2097152 | tf_op jit(solution)/shard_map/all_to_all | solution.py:46
  261.8 0.1 copy.84
  261.9 14.8 %all-to-all-done.4 = bf16[8,256,256]{2,1,0:T(8,128)(2,1)S(1)} async-done(((bf16[8,256,256]{2,1,0:T(8,128)(2,1)}), bf16[8,256,256]{2,1,0:T(8,128)(2,1)S(1)}, u32[]{:S(2)}, u32[]{:S(2)}) %all-to-all-start.4) | async-done | bytes 1048608 | tf_op jit(solution)/shard_map/all_to_all | solution.py:46
  276.7 0.1 convert_reduce_fusion
  276.8 0.7 add_convert_fusion
  (84 shorter events, 1.1 us)
Async XLA Ops:
  6.5 94.0 %copy-start = (bf16[2,64,64]{2,1,0:T(8,128)(2,1)S(1)}, bf16[2,64,64]{2,1,0:T(8,128)(2,1)}, u32[]{:S(2)}) copy-start(bf16[2,64,64]{2,1,0:T(8,128)(2,1)} %param.21) | copy-start | bytes 49156
  6.5 92.2 %all-gather.7.cloned.1.call-start = ((), (), s32[]{:S(2)}) async-start(), calls=%async_computation.5 | async-start | bytes 1064960 | tf_op jit(solution)/shard_map/all_gather | solution.py:35
  7.9 142.8 %all-gather.11.cloned.1.call-start = ((), (), s32[]{:S(2)}) async-start(), calls=%async_computation.7 | async-start | bytes 3538944 | tf_op jit(solution)/shard_map/all_gather | solution.py:53
  36.2 15.1 %copy-start.6 = (bf16[2048]{0:T(1024)(128)(2,1)S(1)}, bf16[2048]{0:T(1024)(128)(2,1)}, u32[]{:S(2)}) copy-start(bf16[2048]{0:T(1024)(128)(2,1)} %param.17) | copy-start | bytes 12292
  36.2 15.1 %copy-start.10 = (f32[128]{0:T(128)S(1)}, f32[128]{0:T(128)}, u32[]{:S(2)}) copy-start(f32[128]{0:T(128)} %param.23) | copy-start | bytes 1540
  36.2 15.1 %copy-start.8 = (bf16[4,128]{1,0:T(4,128)(2,1)S(1)}, bf16[4,128]{1,0:T(4,128)(2,1)}, u32[]{:S(2)}) copy-start(bf16[4,128]{1,0:T(4,128)(2,1)} %param.20) | copy-start | bytes 3076
  36.2 30.1 %copy-start.5 = (bf16[128,32]{0,1:T(8,128)(2,1)S(1)}, bf16[128,32]{0,1:T(8,128)(2,1)}, u32[]{:S(2)}) copy-start(bf16[128,32]{0,1:T(8,128)(2,1)} %param.25) | copy-start | bytes 24580
  36.3 203.7 %all-gather.9.cloned.1.call-start = ((), (), s32[]{:S(2)}) async-start(), calls=%async_computation.6 | async-start | bytes 5857280 | tf_op jit(solution)/shard_map/all_gather | solution.py:35
  40.0 26.3 %all-to-all-start = ((bf16[8,256,256]{1,2,0:T(8,128)(2,1)}), bf16[8,256,256]{1,2,0:T(8,128)(2,1)S(1)}, u32[]{:S(2)}, u32[]{:S(2)}) async-start(bf16[8,256,256]{1,2,0:T(8,128)(2,1)} %broadcast_in_dim.6), calls=%async_computation | async-start | bytes 2097152 | tf_op jit(solution)/shard_map/all_to_all | solution.py:23
  67.1 35.7 %all-to-all-start.1 = ((bf16[64,128,32]{1,2,0:T(8,128)(2,1)}), bf16[64,128,32]{1,2,0:T(8,128)(2,1)S(1)}, u32[]{:S(2)}, u32[]{:S(2)}) async-start(bf16[64,128,32]{1,2,0:T(8,128)(2,1)} %broadcast_in_dim.7), calls=%async_computation.1 | async-start | bytes 1048576 | tf_op jit(solution)/shard_map/all_to_all | solution.py:23
  77.5 23.4 %copy-start.9 = (bf16[2,64,64]{2,1,0:T(8,128)(2,1)S(1)}, bf16[2,64,64]{2,1,0:T(8,128)(2,1)}, u32[]{:S(2)}) copy-start(bf16[2,64,64]{2,1,0:T(8,128)(2,1)} %param.22) | copy-start | bytes 49156
  77.5 23.7 %copy-start.2 = (f32[256,128]{1,0:T(8,128)S(1)}, f32[256,128]{1,0:T(8,128)}, u32[]{:S(2)}) copy-start(f32[256,128]{1,0:T(8,128)} %param.24) | copy-start | bytes 393220
  104.8 24.2 %copy-start.1 = (bf16[256,256]{1,0:T(8,128)(2,1)S(1)}, bf16[256,256]{1,0:T(8,128)(2,1)}, u32[]{:S(2)}) copy-start(bf16[256,256]{1,0:T(8,128)(2,1)} %param.16) | copy-start | bytes 393220
  129.1 5.6 %copy-start.7 = (bf16[2048]{0:T(1024)(128)(2,1)S(1)}, bf16[2048]{0:T(1024)(128)(2,1)}, u32[]{:S(2)}) copy-start(bf16[2048]{0:T(1024)(128)(2,1)} %param.26) | copy-start | bytes 12292
  129.1 5.6 %copy-start.3 = (bf16[3,704]{1,0:T(4,128)(2,1)S(1)}, bf16[3,704]{1,0:T(4,128)(2,1)}, u32[]{:S(2)}) copy-start(bf16[3,704]{1,0:T(4,128)(2,1)} %param.30) | copy-start | bytes 12676
  129.1 5.6 %copy-start.4 = (bf16[3,704]{1,0:T(4,128)(2,1)S(1)}, bf16[3,704]{1,0:T(4,128)(2,1)}, u32[]{:S(2)}) copy-start(bf16[3,704]{1,0:T(4,128)(2,1)} %param.29) | copy-start | bytes 12676
  130.2 19.4 %all-to-all-start.3 = ((bf16[8,256,256]{2,1,0:T(8,128)(2,1)}), bf16[8,256,256]{2,1,0:T(8,128)(2,1)S(1)}, u32[]{:S(2)}, u32[]{:S(2)}) async-start(bf16[8,256,256]{2,1,0:T(8,128)(2,1)} %broadcast_in_dim.8), calls=%async_computation.3 | async-start | bytes 2097152 | tf_op jit(solution)/shard_map/all_to_all | solution.py:23
  253.5 23.2 %all-to-all-start.4 = ((bf16[8,256,256]{2,1,0:T(8,128)(2,1)}), bf16[8,256,256]{2,1,0:T(8,128)(2,1)S(1)}, u32[]{:S(2)}, u32[]{:S(2)}) async-start(bf16[8,256,256]{2,1,0:T(8,128)(2,1)} %bitcast.73), calls=%async_computation.4 | async-start | bytes 2097152 | tf_op jit(solution)/shard_map/all_to_all | solution.py:46
Sparse Core Ops, SparseCore 0:
  10.4 88.3 all-gather.6
  100.8 49.8 all-gather.10
  153.7 86.2 all-gather.8
where the time goes:
time: 285 us; the launch traced here: 284 us
  waiting for transfers between devices  152 us (53%)
  blocking collectives  52.4 us (18%)
  starting transfers between devices  33.9 us (12%)
  matrix products  15.1 us (5%)
  between operations  13.8 us (5%)
  local copies, waits for them, and re-layouts  11.4 us (4%)
  other arithmetic  6 us (2%)
    all_gather x2, waiting for transfers between devices, side_by_side(): result = lax.all_gather(both, axis, axis=dim, tiled=True)  107 us
    all_to_all x3, waiting for transfers between devices, from_everyone(): lax.all_to_all(jnp.broadcast_to(array[None], (size, *array.shape)), axis,...  29.8 us
    all_gather x1, blocking collectives, all_blocks(): parts = lax.all_gather(parts, axes[k])  28.3 us
    all_to_all x3, starting transfers between devices, from_everyone(): lax.all_to_all(jnp.broadcast_to(array[None], (size, *array.shape)), axis,...  25.5 us
    all_to_all x1, blocking collectives, sent_and_summed(): parts = lax.all_to_all(in_blocks(array, dim, size), axis, 0, 0, tiled=True)  24.1 us
    all_to_all x1, waiting for transfers between devices, sent_and_summed(): parts = lax.all_to_all(in_blocks(array, dim, size), axis, 0, 0, tiled=True)  14.8 us
    all_to_all x1, starting transfers between devices, sent_and_summed(): parts = lax.all_to_all(in_blocks(array, dim, size), axis, 0, 0, tiled=True)  8.27 us
  transfers between devices with their start and end apart: 7, of which 6 were waited for; matrix products, arithmetic and copies ran while one was open for 6% of the time, Pallas kernels for 0%

commit v1 on v0

v1 whole, which is shorter than its diff:
```python
import functools

import jax
import jax.numpy as jnp
from jax import lax
from jax.experimental import pallas as pl
from jax.experimental.pallas import tpu as pltpu
from jax.sharding import Mesh
from jax.sharding import PartitionSpec as P

SEQ = 64
FS = ("fs_0", "fs_1")
EPS = 1e-06
DECAY_RATE_GAIN = 8.0
BF = jnp.bfloat16
F32 = jnp.float32
MESH = pl.DeviceIdType.MESH
N = 8
X = 4
MESSAGES = 240


def f32(v):
    return v.astype(F32)


def dot(a, b):
    return jnp.dot(a, b, preferred_element_type=F32)


def dot_t(a, b):
    return lax.dot_general(a, b, (((1,), (1,)), ((), ())), preferred_element_type=F32)


def place(offset):
    r = lax.broadcasted_iota(jnp.int32, (64, 128), 0)
    c = lax.broadcasted_iota(jnp.int32, (64, 128), 1)
    return jnp.where(c == r + offset, 1.0, 0.0).astype(BF)


def shifted(v, k, row, fill=0.0):
    return jnp.where(row >= k, pltpu.roll(v, k, 0), fill)


def conv(v, taps, row):
    width = taps.shape[0]
    total = v * taps[width - 1 : width]
    for k in range(1, width):
        total = total + shifted(v, k, row) * taps[width - 1 - k : width - k]
    return total


class Wire:
    def __init__(self, send, recv):
        self.send_sem, self.recv_sem, self.copies = send, recv, {}

    def go(self, key, src, dst, dev):
        k = len(self.copies)
        copy = pltpu.make_async_remote_copy(
            src_ref=src,
            dst_ref=dst,
            send_sem=self.send_sem.at[k],
            recv_sem=self.recv_sem.at[k],
            device_id=dev,
            device_id_type=MESH,
        )
        copy.start()
        self.copies[key] = copy

    def got(self, key):
        self.copies[key].wait_recv()

    def finish(self):
        for copy in self.copies.values():
            copy.wait_send()


class Spread:
    def __init__(self, wire, name, index, buf, chunks, here):
        self.wire, self.name, self.index, self.buf, self.chunks = wire, name, index, buf, chunks
        self.z, self.y, self.t = here

    def neighbour(self, axis, way):
        if axis == 0:
            return (lax.rem(self.z + N + way, N), self.y, self.t)
        return (self.z, lax.rem(self.y + N + way, N), self.t)

    def first(self, half, way, step):
        axis = 1 - half
        pos = lax.rem((self.y if axis else self.z) + N - way * (step - 1), N)
        return self.buf.at[self.z, pos, 0] if half == 0 else self.buf.at[pos, self.y, 1]

    def steps1(self, half, way):
        far = 1 if (self.index + half) % 2 == 0 else -1
        return N // 2 if way == far else N // 2 - 1

    def send1(self, step):
        for half in (0, 1):
            for way in (1, -1):
                if step <= self.steps1(half, way):
                    ref = self.first(half, way, step)
                    self.wire.go((self.name, 1, half, way, step), ref, ref, self.neighbour(1 - half, way))

    def forward1(self, step):
        for half in (0, 1):
            for way in (1, -1):
                if step <= self.steps1(half, way):
                    self.wire.got((self.name, 1, half, way, step))
                if step + 1 <= self.steps1(half, way):
                    ref = self.first(half, way, step + 1)
                    self.wire.go(
                        (self.name, 1, half, way, step + 1), ref, ref, self.neighbour(1 - half, way)
                    )

    def second(self, half, way, step, q):
        size = N // self.chunks
        pos = lax.rem((self.y if half else self.z) + N - way * (step - 1), N)
        part = pl.ds(q * size, size)
        return self.buf.at[pos, part, 0] if half == 0 else self.buf.at[part, pos, 1]

    def steps2(self, way, q):
        far = 1 if q < self.chunks // 2 else -1
        return N // 2 if way == far else N // 2 - 1

    def send2(self, q):
        for half in (0, 1):
            for way in (1, -1):
                ref = self.second(half, way, 1, q)
                self.wire.go((self.name, 2, half, way, 1, q), ref, ref, self.neighbour(half, way))

    def forward2(self, q, step):
        for half in (0, 1):
            for way in (1, -1):
                if step <= self.steps2(way, q):
                    self.wire.got((self.name, 2, half, way, step, q))
                if step + 1 <= self.steps2(way, q):
                    ref = self.second(half, way, step + 1, q)
                    self.wire.go(
                        (self.name, 2, half, way, step + 1, q), ref, ref, self.neighbour(half, way)
                    )


class Row:
    def __init__(self, z, y, t):
        self.z, self.y, self.t = z, y, t
        self.x, self.c = t // 2, lax.rem(t, 2)
        self.right = lax.rem(self.x + 1, X)
        self.left = lax.rem(self.x + X - 1, X)
        self.across = lax.rem(self.x + 2, X)

    def dev(self, x):
        return (self.z, self.y, 2 * x + self.c)

    def same(self, x):
        return 2 * x + self.c

    @property
    def partner(self):
        return (self.z, self.y, 2 * self.x + 1 - self.c)


class Gather:
    def __init__(self, wire, name, buf, row):
        self.wire, self.name, self.buf, self.row = wire, name, buf, row

    def key(self, *k):
        return (self.name, *k)

    def start(self):
        r, b = self.row, self.buf
        for k in (0, 1):
            for way, x in ((1, r.right), (-1, r.left)):
                half = k if way == 1 else 1 - k
                ref = b.at[r.t, half]
                self.wire.go(self.key("near", way, half), ref, ref, r.dev(x))
        self.wire.go(self.key("own"), b.at[r.t], b.at[r.t], r.partner)

    def relay(self):
        r, b = self.row, self.buf
        self.wire.got(self.key("near", 1, 0))
        ref = b.at[r.same(r.left), 0]
        self.wire.go(self.key("far", 1), ref, ref, r.dev(r.right))
        self.wire.got(self.key("near", -1, 1))
        ref = b.at[r.same(r.right), 1]
        self.wire.go(self.key("far", -1), ref, ref, r.dev(r.left))

    def share(self):
        r, b = self.row, self.buf
        self.wire.got(self.key("near", 1, 1))
        ref = b.at[r.same(r.left)]
        self.wire.go(self.key("left"), ref, ref, r.partner)
        self.wire.got(self.key("near", -1, 0))
        ref = b.at[r.same(r.right)]
        self.wire.go(self.key("right"), ref, ref, r.partner)

    def share_far(self):
        r, b = self.row, self.buf
        self.wire.got(self.key("far", 1))
        self.wire.got(self.key("far", -1))
        ref = b.at[r.same(r.across)]
        self.wire.go(self.key("across"), ref, ref, r.partner)

    def done(self):
        for k in ("own", "left", "right", "across"):
            self.wire.got(self.key(k))


class Sum:
    def __init__(self, wire, name, row, part, pair, stage, mid, end):
        self.wire, self.name, self.row = wire, name, row
        self.part, self.pair, self.stage, self.mid, self.end = part, pair, stage, mid, end

    def start(self):
        r = self.row
        self.wire.go((self.name, "pair"), self.part.at[1 - r.c], self.pair, r.partner)

    def both(self, x, half):
        rows = pl.ds(half * 128, 128)
        return f32(self.part[self.row.c, x, rows, :]) + f32(self.pair[x, rows, :])

    def out(self, k, value, dst, way):
        r = self.row
        self.stage[k] = value.astype(BF)
        self.wire.go((self.name, k), self.stage.at[k], dst, r.dev(r.right if way == 1 else r.left))

    def spread(self):
        r = self.row
        self.wire.got((self.name, "pair"))
        self.out(0, self.both(r.across, 0), self.mid.at[0], 1)
        self.out(1, self.both(r.across, 1), self.mid.at[1], -1)
        self.out(2, self.both(r.right, 1), self.end.at[0, 1], 1)
        self.out(3, self.both(r.left, 0), self.end.at[1, 0], -1)

    def relay(self):
        r = self.row
        self.wire.got((self.name, 0))
        self.out(4, self.both(r.right, 0) + f32(self.mid[0]), self.end.at[0, 0], 1)
        self.wire.got((self.name, 1))
        self.out(5, self.both(r.left, 1) + f32(self.mid[1]), self.end.at[1, 1], -1)

    def total(self, half):
        r = self.row
        if half == 0:
            for k in (2, 3, 4, 5):
                self.wire.got((self.name, k))
        return self.both(r.x, half) + f32(self.end[0, half]) + f32(self.end[1, half])


def normed_into(out, buf, gain):
    for half in (0, 1):
        for part in (0, 1):
            rows = pl.ds(part * 64, 64)
            sums = jnp.zeros((64, 256), F32)
            for j in range(N):
                v = f32(buf[j, half, rows, :])
                sums = sums + v * v
            mean = jnp.sum(sums, axis=1, keepdims=True) * (1.0 / (N * 256))
            factor = lax.rsqrt(mean + EPS)
            for j in range(N):
                v = f32(buf[j, half, rows, :])
                cols = pl.ds(j * 256, 256)
                out[pl.ds(half * 128 + part * 64, 64), cols] = (
                    v * factor * f32(gain[:, cols])
                ).astype(BF)


def kernel(
    tok,
    gain1,
    wb,
    wg,
    taps1,
    rmap,
    imap,
    rate,
    pld,
    wo,
    gain2,
    ug,
    uv,
    gtaps,
    vtaps,
    dn,
    out,
    gm,
    gu,
    gd,
    tokb,
    aftb,
    nrm,
    mixed,
    gv,
    hid,
    part1,
    pair1,
    stage1,
    mid1,
    end1,
    part2,
    pair2,
    stage2,
    mid2,
    end2,
    ssem,
    rsem,
):
    z, y, t = lax.axis_index("fs_0"), lax.axis_index("fs_1"), lax.axis_index("tp")
    here = (z, y, t)
    wire = Wire(ssem, rsem)
    row = Row(z, y, t)
    mix = Spread(wire, "mix", 0, gm, 2, here)
    up = Spread(wire, "up", 1, gu, 4, here)
    down = Spread(wire, "down", 2, gd, 2, here)
    ag1 = Gather(wire, "tok", tokb, row)
    ag2 = Gather(wire, "aft", aftb, row)
    rs1 = Sum(wire, "rs1", row, part1, pair1, stage1, mid1, end1)
    rs2 = Sum(wire, "rs2", row, part2, pair2, stage2, mid2, end2)

    barrier = pltpu.get_barrier_semaphore()
    peers = [
        mix.neighbour(0, 1),
        mix.neighbour(0, -1),
        mix.neighbour(1, 1),
        mix.neighbour(1, -1),
        row.dev(row.right),
        row.dev(row.left),
        row.partner,
    ]
    for peer in peers:
        pl.semaphore_signal(barrier, inc=1, device_id=peer, device_id_type=MESH)

    split = (2, 16)
    gm[z, y, :, :, 0:128] = wb[...].reshape(*split, 128)
    gm[z, y, :, :, 128:256] = wg[...].reshape(*split, 128)
    gm[z, y, :, :, 256:384] = wo[...].reshape(*split, 128)
    low, high = place(0), place(64)
    tokb[t] = tok[...].reshape(2, 128, 256)
    gu[z, y, :, :, 0:640] = ug[:, 0:640].reshape(*split, 640)
    gu[z, y, :, :, 640:1280] = uv[:, 0:640].reshape(*split, 640)
    tail = dot(ug[:, 640:704], low) + dot(uv[:, 640:704], high)
    gu[z, y, :, :, 1280:1408] = tail.astype(BF).reshape(*split, 128)
    gd[z, y, :, :, 0:640] = dn[:, 0:640].reshape(*split, 640)
    gd[z, y, :, :, 640:768] = dot(dn[:, 640:704], low).astype(BF).reshape(*split, 128)

    pl.semaphore_wait(barrier, len(peers))

    mix.send1(1)
    ag1.start()
    up.send1(1)
    down.send1(1)
    mix.forward1(1)
    up.forward1(1)
    mix.forward1(2)
    ag1.relay()
    down.forward1(1)
    mix.forward1(3)
    ag1.share()
    up.forward1(2)
    mix.forward1(4)
    mix.send2(0)
    mix.send2(1)
    ag1.share_far()
    up.forward1(3)
    down.forward1(2)
    up.forward1(4)
    up.send2(0)
    mix.forward2(0, 1)
    mix.forward2(1, 1)
    up.send2(1)
    down.forward1(3)
    ag1.done()
    normed_into(nrm, tokb, gain1)
    mix.forward2(0, 2)
    mix.forward2(1, 2)
    up.send2(2)
    up.forward2(0, 1)
    mix.forward2(0, 3)
    mix.forward2(1, 3)
    up.send2(3)
    up.forward2(1, 1)
    down.forward1(4)
    mix.forward2(0, 4)
    mix.forward2(1, 4)
    up.forward2(2, 1)

    both = dot(nrm[...], gm[:, :, :, :, 0:256].reshape(2048, 256))
    branch = both[:, 0:128].astype(BF)
    outgate = both[:, 128:256].astype(BF)
    up.forward2(0, 2)
    up.forward2(3, 1)
    rmat = jnp.concatenate([dot(rmap[0], low), dot(rmap[1], high)], axis=0).astype(BF)
    imat = jnp.concatenate([dot(imap[0], low), dot(imap[1], high)], axis=0).astype(BF)
    pos = lax.broadcasted_iota(jnp.int32, (SEQ, 128), 0)
    ctaps = f32(taps1[...])
    for s in range(4):
        rows = slice(s * SEQ, (s + 1) * SEQ)
        cv = conv(f32(branch[rows]), ctaps, pos).astype(BF)
        recur = jax.nn.sigmoid(dot(cv, rmat))
        inner = jax.nn.sigmoid(dot(cv, imat))
        loga = -DECAY_RATE_GAIN * recur * rate[...] + pld[rows, :]
        a = jnp.exp(loga)
        d = jnp.sqrt(jnp.tanh(-loga) * (1.0 + a * a)) * inner * f32(cv)
        k = 1
        while k < SEQ:
            d = d + a * shifted(d, k, pos)
            if 2 * k < SEQ:
                a = a * shifted(a, k, pos, 1.0)
            k *= 2
        mixed[rows, :] = (d * jax.nn.gelu(f32(outgate[rows]))).astype(BF)
    up.forward2(1, 2)
    for j in range(N):
        w = gm[j, :, :, :, 256:384].reshape(256, 128)
        part1[j % 2, j // 2] = dot_t(mixed[...], w).astype(BF)
    rs1.start()
    up.forward2(2, 2)
    rs1.spread()
    up.forward2(3, 2)
    down.send2(0)
    up.forward2(0, 3)
    rs1.relay()
    up.forward2(1, 3)
    for half in (0, 1):
        rows = pl.ds(half * 128, 128)
        aftb[t, half] = (f32(tok[rows, :]) + rs1.total(half)).astype(BF)
    ag2.start()
    up.forward2(2, 3)
    down.send2(1)
    ag2.relay()
    up.forward2(3, 3)
    ag2.share()
    down.forward2(0, 1)
    ag2.share_far()
    up.forward2(0, 4)
    up.forward2(1, 4)
    ag2.done()
    normed_into(nrm, aftb, gain2)
    down.forward2(1, 1)
    up.forward2(2, 4)
    up.forward2(3, 4)

    for k in range(6):
        cols = pl.ds(k * 256, 256 if k < 5 else 128)
        w = gu[:, :, :, :, cols]
        gv[:, cols] = dot(nrm[...], w.reshape(2048, w.shape[-1])).astype(BF)
        if k == 2:
            down.forward2(0, 2)
        if k == 4:
            down.forward2(1, 2)
    tail_taps = dot(gtaps[:, 640:704], low) + dot(vtaps[:, 640:704], high)
    lane = lax.broadcasted_iota(jnp.int32, (SEQ, 128), 1)
    for s in range(4):
        rows = pl.ds(s * SEQ, SEQ)
        for k in range(5):
            cols = pl.ds(k * 128, 128)
            g = conv(f32(gv[rows, cols]), f32(gtaps[:, cols]), pos)
            v = conv(f32(gv[rows, pl.ds(640 + k * 128, 128)]), f32(vtaps[:, cols]), pos)
            hid[rows, cols] = (jax.nn.silu(g) * v).astype(BF)
        b = conv(f32(gv[rows, pl.ds(1280, 128)]), tail_taps, pos)
        h = jnp.where(lane < 64, jax.nn.silu(b) * pltpu.roll(b, 64, 1), 0.0)
        hid[rows, pl.ds(640, 128)] = h.astype(BF)
    down.forward2(0, 3)
    down.forward2(1, 3)
    down.forward2(0, 4)
    down.forward2(1, 4)
    for j in range(N):
        w = gd[j].reshape(256, 768)
        part2[j % 2, j // 2] = dot_t(hid[...], w).astype(BF)
    rs2.start()
    rs2.spread()
    rs2.relay()
    for half in (0, 1):
        rows = pl.ds(half * 128, 128)
        out[rows, :] = (f32(aftb[t, half]) + rs2.total(half)).astype(BF)
    wire.finish()


def per_device(*args):
    (tok, gain1, wb, wg, taps1, rmap, imap, rate, pld, wo, gain2, ug, uv, gtaps, vtaps, dn) = args
    sums = [
        pltpu.VMEM((2, X, 256, 256), BF),
        pltpu.VMEM((X, 256, 256), BF),
        pltpu.VMEM((6, 128, 256), BF),
        pltpu.VMEM((2, 128, 256), BF),
        pltpu.VMEM((2, 2, 128, 256), BF),
    ]
    return pl.pallas_call(
        kernel,
        out_shape=jax.ShapeDtypeStruct((256, 256), BF),
        in_specs=[pl.BlockSpec(memory_space=pltpu.VMEM)] * 16,
        out_specs=pl.BlockSpec(memory_space=pltpu.VMEM),
        scratch_shapes=[
            pltpu.VMEM((N, N, 2, 16, 384), BF),
            pltpu.VMEM((N, N, 2, 16, 1408), BF),
            pltpu.VMEM((N, N, 2, 16, 768), BF),
            pltpu.VMEM((N, 2, 128, 256), BF),
            pltpu.VMEM((N, 2, 128, 256), BF),
            pltpu.VMEM((256, 2048), BF),
            pltpu.VMEM((256, 128), BF),
            pltpu.VMEM((256, 1408), BF),
            pltpu.VMEM((256, 768), BF),
            *sums,
            *sums,
            pltpu.SemaphoreType.DMA((MESSAGES,)),
            pltpu.SemaphoreType.DMA((MESSAGES,)),
        ],
        compiler_params=pltpu.CompilerParams(
            collective_id=0, has_side_effects=True, vmem_limit_bytes=48 * 2**20
        ),
        name="layer",
    )(
        tok,
        gain1.reshape(1, -1),
        wb,
        wg,
        taps1,
        rmap,
        imap,
        rate.reshape(1, -1),
        pld,
        wo.T,
        gain2.reshape(1, -1),
        ug,
        uv,
        gtaps,
        vtaps,
        dn.T,
    )


def solution(mesh):
    torus = Mesh(mesh.devices.reshape(N, N, mesh.shape["tp"]), ("fs_0", "fs_1", "tp"))
    return jax.shard_map(
        per_device,
        mesh=torus,
        in_specs=(
            P(FS, "tp"),
            P(),
            P(FS, "tp"),
            P(FS, "tp"),
            P(None, "tp"),
            P("tp", None, None),
            P("tp", None, None),
            P("tp"),
            P(FS, "tp"),
            P("tp", FS),
            P(),
            P(FS, "tp"),
            P(FS, "tp"),
            P(None, "tp"),
            P(None, "tp"),
            P("tp", FS),
        ),
        out_specs=P(FS, "tp"),
        check_vma=False,
    )
```

time: 285 us -> 110 us (0.39)
  waiting for transfers between devices: 152 us -> 0 us
  Pallas kernels: 0 us -> 100 us
  blocking collectives: 52.4 us -> 0 us
  starting transfers between devices: 33.9 us -> 0 us
  matrix products: 15.1 us -> 0 us
  between operations: 13.8 us -> 0.08 us
  other arithmetic: 6 us -> 0 us
    all_gather x3 -> x0, waiting for transfers between devices: 107 us -> none  [the longest x2 107 us: side_by_side(): result = lax.all_gather(both, axis, axis=dim, tiled=True)]
    pallas_call x0 -> x1, Pallas kernels: none -> 100 us  [per_device(): pl.pallas_call(kernel, out_shape=jax.ShapeDtypeStruct((256, 256), BF), in...]
    all_to_all x4 -> x0, waiting for transfers between devices: 44.7 us -> none  [the longest x3 29.8 us: from_everyone(): lax.all_to_all(jnp.broadcast_to(array[None], (size, *array.shape)), axis,...]
    all_to_all x4 -> x0, starting transfers between devices: 33.8 us -> none  [the longest x3 25.5 us: from_everyone(): lax.all_to_all(jnp.broadcast_to(array[None], (size, *array.shape)), axis,...]
    all_gather x1 -> x0, blocking collectives: 28.3 us -> none  [all_blocks(): parts = lax.all_gather(parts, axes[k])]
    all_to_all x1 -> x0, blocking collectives: 24.1 us -> none  [sent_and_summed(): parts = lax.all_to_all(in_blocks(array, dim, size), axis, 0, 0, tiled=True)]
    dot_general x7 -> x0, matrix products: 15.1 us -> none  [the longest x1 4.86 us: per_device(): jnp.dot(normed2, value_whole, preferred_element_type=jnp.float32)]
    unnamed x24 -> x31, local copies, waits for them, and re-layouts: 1.16 us -> 8.45 us
  transfers between devices with their start and end apart: 7 -> 0, of which waited for: 6 -> 0; matrix products, arithmetic and copies ran while one was open for 6% -> 0% of each run, Pallas kernels for 0% -> 0%
where the time goes in v1:
time: 110 us; the launch traced here: 109 us
  Pallas kernels  100 us (91%)
  local copies, waits for them, and re-layouts  9.17 us (8%)
    pallas_call x1, Pallas kernels, per_device(): pl.pallas_call(kernel, out_shape=jax.ShapeDtypeStruct((256, 256), BF), in...  100 us
    unnamed x31, local copies, waits for them, and re-layouts  8.45 us

profile of v1, /device:TPU:1, one launch (start us, length us, event | category | flops | bytes accessed | tf_op | source)
XLA Modules:
  0.0 109.4 jit_solution(946257409548757260)
XLA Ops:
  0.0 0.0 copy-start.14
  0.0 0.0 copy-start.12
  0.0 0.0 copy-start.13
  0.0 0.7 copy-done.14
  0.7 0.0 copy-start.8
  0.7 0.0 copy-start.9
  0.7 0.0 copy-start.7
  0.7 0.7 reshape.11.gain2
  1.4 0.0 copy-done.12
  1.4 0.0 copy-done.13
  1.4 0.0 copy-done.8
  1.5 0.0 copy-done.9
  1.5 0.0 copy-done.7
  1.5 0.0 copy-start
  1.5 0.9 copy-done
  2.4 0.0 copy-start.1
  2.4 0.9 copy-done.1
  3.3 0.0 copy-start.2
  3.3 0.8 copy-done.2
  4.1 0.0 copy-start.3
  4.1 0.8 copy-done.3
  4.9 0.0 copy-start.4
  4.9 0.8 copy-done.4
  5.7 0.0 copy-start.5
  5.7 0.8 copy-done.5
  6.4 0.0 copy-start.6
  6.4 0.8 copy-done.6
  7.2 0.0 copy-start.10
  7.2 0.7 copy-done.10
  7.9 0.0 copy-start.11
  7.9 0.7 copy-done.11
  8.6 100.1 %layer.1 = bf16[256,256]{1,0:T(8,128)(2,1)S(1)} custom-call(bf16[256,256]{1,0:T(8,128)(2,1)S(1)} %copy-done, bf16[1,2048]{1,0:T(2,128)(2,1)S(1)} %reshape.9.gain1, bf16[32,128]{1,0:T(8,128)(2,1)S(1)} %copy-done.7, bf16[32,128]{1,0:T(8,128)(2,1)S(1)} %copy-done.8, bf16[4,128]{1,0:T(4,128)(2,1)S(1)} %copy-done.12, bf16[2,64,64]{2,1,0:T(8,128)(2,1)S(1)} %copy-done.5, ...), custom_call_target="tpu_custom_call" | custom-call | tf_op jit(solution)/shard_map/layer/pallas_call | solution.py:486
  108.7 0.7 copy.18
  (1 shorter events, 0.0 us)
Async XLA Ops:
  0.0 0.7 copy-start.14
  0.0 1.4 %copy-start.12 = (bf16[4,128]{1,0:T(4,128)(2,1)S(1)}, bf16[4,128]{1,0:T(4,128)(2,1)}, u32[]{:S(2)}) copy-start(bf16[4,128]{1,0:T(4,128)(2,1)} %taps1.1) | copy-start | bytes 3076
  0.0 1.4 %copy-start.13 = (f32[128]{0:T(128)S(1)}, f32[128]{0:T(128)}, u32[]{:S(2)}) copy-start(f32[128]{0:T(128)} %param.23) | copy-start | bytes 1540
  0.7 0.8 copy-start.8
  0.7 0.8 copy-start.9
  0.7 0.8 copy-start.7
  1.5 0.9 copy-start
  2.4 0.9 copy-start.1
  3.3 0.8 copy-start.2
  4.1 0.8 copy-start.3
  4.9 0.8 copy-start.4
  5.7 0.8 copy-start.5
  6.4 0.8 copy-start.6
  7.2 0.7 copy-start.10
  7.9 0.7 copy-start.11

commit v2 on v1

v2 whole, which is shorter than its diff:
```python
import functools

import jax
import jax.numpy as jnp
from jax import lax
from jax.experimental import pallas as pl
from jax.experimental.pallas import tpu as pltpu
from jax.sharding import Mesh
from jax.sharding import PartitionSpec as P

SEQ = 64
FS = ("fs_0", "fs_1")
EPS = 1e-06
DECAY_RATE_GAIN = 8.0
BF = jnp.bfloat16
F32 = jnp.float32
MESH = pl.DeviceIdType.MESH
N = 8
X = 4
SENDS = 14
ARRIVALS = 100
CHUNKS = (4, 8, 4)
ORDER = (
    ("mix", "s1"),
    ("ag1", "start", 0),
    ("up", "s1"),
    ("up", "s2", 0),
    ("dn", "s1"),
    ("mix", "f1", 1),
    ("mix", "s2", 0),
    ("up", "f1", 1),
    ("up", "s2", 7),
    ("dn", "f1", 1),
    ("mix", "f1", 2),
    ("up", "s2", 1),
    ("up", "f2", 0, 1),
    ("up", "f1", 2),
    ("mix", "f2", 0, 1),
    ("ag1", "relay", 0),
    ("mix", "f1", 3),
    ("mix", "s2", 1),
    ("up", "s2", 2),
    ("mix", "s2", 3),
    ("dn", "f1", 2),
    ("up", "f2", 7, 1),
    ("mix", "f1", 4),
    ("mix", "s2", 2),
    ("mix", "f2", 1, 1),
    ("up", "f1", 3),
    ("dn", "s2", 0),
    ("mix", "f2", 3, 1),
    ("ag1", "share", 0),
    ("up", "f2", 2, 1),
    ("ag1", "sharefar", 0),
    ("mix", "f2", 2, 1),
    ("mix", "f2", 0, 2),
    ("up", "f2", 1, 1),
    ("mix", "f2", 1, 2),
    ("up", "s2", 3),
    ("up", "f2", 0, 2),
    ("mix", "f2", 2, 2),
    ("up", "f1", 4),
    ("mix", "f2", 3, 2),
    ("ag1", "done", 0),
    ("up", "s2", 4),
    ("dn", "f1", 3),
    ("up", "s2", 5),
    ("mix", "f2", 1, 3),
    ("norm1",),
    ("up", "s2", 6),
    ("mix", "f2", 0, 3),
    ("mix", "f2", 2, 3),
    ("mix", "f2", 3, 3),
    ("up", "f2", 4, 1),
    ("dn", "f1", 4),
    ("dn", "s2", 3),
    ("up", "f2", 3, 1),
    ("up", "f2", 1, 2),
    ("up", "f2", 5, 1),
    ("mix", "f2", 0, 4),
    ("mix", "f2", 3, 4),
    ("up", "f2", 7, 2),
    ("mix", "f2", 1, 4),
    ("up", "f2", 2, 2),
    ("up", "f2", 0, 3),
    ("mix", "f2", 2, 4),
    ("win",),
    ("mixer",),
    ("part1", 0),
    ("rs1", "start", 0),
    ("up", "f2", 6, 1),
    ("part1", 1),
    ("rs1", "start", 1),
    ("dn", "s2", 1),
    ("rs1", "spread", 0),
    ("up", "f2", 3, 2),
    ("dn", "s2", 2),
    ("up", "f2", 4, 2),
    ("rs1", "spread", 1),
    ("rs1", "relay", 0),
    ("up", "f2", 5, 2),
    ("rs1", "relay", 1),
    ("up", "f2", 6, 2),
    ("up", "f2", 7, 3),
    ("dn", "f2", 1, 1),
    ("rs1", "total", 0),
    ("up", "f2", 1, 3),
    ("ag2", "start", 0),
    ("up", "f2", 3, 3),
    ("dn", "f2", 0, 1),
    ("rs1", "total", 1),
    ("ag2", "start", 1),
    ("up", "f2", 4, 3),
    ("up", "f2", 5, 3),
    ("up", "f2", 6, 3),
    ("dn", "f2", 3, 1),
    ("up", "f2", 2, 3),
    ("dn", "f2", 2, 1),
    ("ag2", "relay", 0),
    ("ag2", "relay", 1),
    ("ag2", "share", 1),
    ("ag2", "share", 0),
    ("dn", "f2", 0, 2),
    ("up", "f2", 5, 4),
    ("ag2", "sharefar", 0),
    ("dn", "f2", 1, 2),
    ("dn", "f2", 3, 2),
    ("up", "f2", 1, 4),
    ("ag2", "sharefar", 1),
    ("up", "f2", 4, 4),
    ("up", "f2", 7, 4),
    ("up", "f2", 3, 4),
    ("up", "f2", 6, 4),
    ("up", "f2", 2, 4),
    ("dn", "f2", 2, 2),
    ("ag2", "done", 0),
    ("dn", "f2", 0, 3),
    ("ag2", "done", 1),
    ("norm2",),
    ("up", "f2", 0, 4),
    ("updot", 1),
    ("dn", "f2", 1, 3),
    ("updot", 3),
    ("dn", "f2", 3, 3),
    ("updot", 0),
    ("dn", "f2", 2, 3),
    ("updot", 5),
    ("updot", 2),
    ("updot", 4),
    ("dn", "f2", 1, 4),
    ("dn", "f2", 0, 4),
    ("hid",),
    ("dn", "f2", 3, 4),
    ("dn", "f2", 2, 4),
    ("part2",),
    ("rs2", "start", 0),
    ("rs2", "start", 1),
    ("rs2", "spread", 0),
    ("rs2", "spread", 1),
    ("rs2", "relay", 0),
    ("rs2", "relay", 1),
    ("rs2", "total", 0),
    ("rs2", "total", 1),
)
FIRST = (2, 3, 9, 0, 11, 12, 15)


def f32(v):
    return v.astype(F32)


def dot(a, b):
    return jnp.dot(a, b, preferred_element_type=F32)


def dot_t(a, b):
    return lax.dot_general(a, b, (((1,), (1,)), ((), ())), preferred_element_type=F32)


def place(offset):
    r = lax.broadcasted_iota(jnp.int32, (64, 128), 0)
    c = lax.broadcasted_iota(jnp.int32, (64, 128), 1)
    return jnp.where(c == r + offset, 1.0, 0.0).astype(BF)


def shifted(v, k, row, fill=0.0):
    return jnp.where(row >= k, pltpu.roll(v, k, 0), fill)


def conv(v, taps, row):
    width = taps.shape[0]
    total = v * taps[width - 1 : width]
    for k in range(1, width):
        total = total + shifted(v, k, row) * taps[width - 1 - k : width - k]
    return total


class Wire:
    def __init__(self, send, recv):
        self.send, self.recv, self.sent, self.due = send, recv, {}, {}

    def go(self, group, key, src, dst, dev):
        out = self.sent.setdefault(group, len(self.sent))
        into = self.due.setdefault(key, len(self.due))
        pltpu.make_async_remote_copy(
            src_ref=src,
            dst_ref=dst,
            send_sem=self.send.at[out],
            recv_sem=self.recv.at[into],
            device_id=dev,
            device_id_type=MESH,
        ).start()

    def got(self, key, ref):
        pltpu.make_async_copy(ref, ref, self.recv.at[self.due[key]]).wait()

    def gone(self, group, ref):
        pltpu.make_async_copy(ref, ref, self.send.at[self.sent[group]]).wait()


class Spread:
    def __init__(self, wire, name, index, buf, chunks, here):
        self.wire, self.name, self.index, self.buf, self.chunks = wire, name, index, buf, chunks
        self.z, self.y, self.t = here

    def neighbour(self, axis, way):
        if axis == 0:
            return (lax.rem(self.z + N + way, N), self.y, self.t)
        return (self.z, lax.rem(self.y + N + way, N), self.t)

    def first(self, half, way, step):
        axis = 1 - half
        pos = lax.rem((self.y if axis else self.z) + N - way * (step - 1), N)
        return self.buf.at[self.z, pos, 0] if half == 0 else self.buf.at[pos, self.y, 1]

    def pass1(self, step):
        for half in (0, 1):
            for way in (1, -1):
                far = 1 if (self.index + half) % 2 == 0 else -1
                if step < N // 2 or (step == N // 2 and way == far):
                    ref = self.first(half, way, step)
                    dev = self.neighbour(1 - half, way)
                    self.wire.go(self.name, (self.name, step), ref, ref, dev)

    def forward1(self, step):
        self.wire.got((self.name, step), self.buf.at[0, pl.ds(0, 2 if step < N // 2 else 1)])
        self.pass1(step + 1)

    def second(self, half, way, step, q):
        size = N // self.chunks
        own = (self.z if half else self.y) // size
        part = pl.ds(lax.rem(own + q, self.chunks) * size, size)
        pos = lax.rem((self.y if half else self.z) + N - way * (step - 1), N)
        return self.buf.at[pos, part, 0] if half == 0 else self.buf.at[part, pos, 1]

    def pass2(self, q, step):
        far = 1 if q < self.chunks // 2 else -1
        for half in (0, 1):
            for way in (1, -1):
                if step < N // 2 or (step == N // 2 and way == far):
                    ref = self.second(half, way, step, q)
                    dev = self.neighbour(half, way)
                    self.wire.go(self.name, (self.name, step, q), ref, ref, dev)

    def forward2(self, q, step):
        size = N // self.chunks
        self.wire.got(
            (self.name, step, q), self.buf.at[0, pl.ds(0, 2 * size if step < N // 2 else size)]
        )
        self.pass2(q, step + 1)

    def finish(self):
        self.wire.gone(self.name, self.buf.reshape(N * N, *self.buf.shape[2:]).at[pl.ds(0, N * N - 1)])


class Row:
    def __init__(self, z, y, t):
        self.z, self.y, self.t = z, y, t
        self.x, self.c = t // 2, lax.rem(t, 2)
        self.right = lax.rem(self.x + 1, X)
        self.left = lax.rem(self.x + X - 1, X)
        self.across = lax.rem(self.x + 2, X)

    def dev(self, x):
        return (self.z, self.y, 2 * x + self.c)

    def same(self, x):
        return 2 * x + self.c

    @property
    def partner(self):
        return (self.z, self.y, 2 * self.x + 1 - self.c)


class Gather:
    def __init__(self, wire, name, buf, row):
        self.wire, self.name, self.buf, self.row = wire, name, buf, row

    def go(self, key, ref, dev):
        self.wire.go(self.name, (self.name, key), ref, ref, dev)

    def got(self, key, count):
        self.wire.got((self.name, key), self.buf.at[pl.ds(0, count)])

    def start(self):
        r, b = self.row, self.buf
        for k in (0, 1):
            self.go(k, b.at[r.t, k], r.dev(r.right))
            self.go(k, b.at[r.t, 1 - k], r.dev(r.left))
        self.go("pair", b.at[r.t], r.partner)

    def relay(self):
        r, b = self.row, self.buf
        self.got(0, 1)
        self.go("far", b.at[r.same(r.left), 0], r.dev(r.right))
        self.go("far", b.at[r.same(r.right), 1], r.dev(r.left))

    def share(self):
        r, b = self.row, self.buf
        self.got(1, 1)
        self.go("pair", b.at[r.same(r.left)], r.partner)
        self.go("pair", b.at[r.same(r.right)], r.partner)

    def share_far(self):
        r, b = self.row, self.buf
        self.got("far", 1)
        self.go("pair", b.at[r.same(r.across)], r.partner)

    def done(self):
        self.got("pair", 4)

    def finish(self):
        self.wire.gone(self.name, self.buf.at[pl.ds(0, 7)])


class Sum:
    def __init__(self, wire, name, row, part, pair, stage, mid, end):
        self.wire, self.name, self.row = wire, name, row
        self.part, self.pair, self.stage, self.mid, self.end = part, pair, stage, mid, end

    def key(self, k):
        return (self.name, k)

    def start(self):
        r = self.row
        self.wire.go(self.key(0), self.key(0), self.part.at[1 - r.c], self.pair, r.partner)

    def both(self, x, half):
        rows = pl.ds(half * 128, 128)
        return f32(self.part[self.row.c, x, rows, :]) + f32(self.pair[x, rows, :])

    def out(self, k, value, dst, way):
        r = self.row
        self.stage[k] = value.astype(BF)
        dev = r.dev(r.right if way == 1 else r.left)
        self.wire.go(self.key(1), self.key(1 if k < 2 else 2), self.stage.at[k], dst, dev)

    def spread(self):
        r = self.row
        self.wire.got(self.key(0), self.pair)
        self.out(0, self.both(r.across, 0), self.mid.at[0], 1)
        self.out(1, self.both(r.across, 1), self.mid.at[1], -1)
        self.out(2, self.both(r.right, 1), self.end.at[0, 1], 1)
        self.out(3, self.both(r.left, 0), self.end.at[1, 0], -1)

    def relay(self):
        r = self.row
        self.wire.got(self.key(1), self.mid)
        self.out(4, self.both(r.right, 0) + f32(self.mid[0]), self.end.at[0, 0], 1)
        self.out(5, self.both(r.left, 1) + f32(self.mid[1]), self.end.at[1, 1], -1)

    def total(self, half):
        r = self.row
        if half == 0:
            self.wire.got(self.key(2), self.end)
        return self.both(r.x, half) + f32(self.end[0, half]) + f32(self.end[1, half])

    def finish(self):
        self.wire.gone(self.key(0), self.pair)
        self.wire.gone(self.key(1), self.stage)


def normed_into(out, bufs, gain):
    width = 256 // len(bufs)
    for half in (0, 1):
        for part in (0, 1):
            rows = pl.ds(part * 64, 64)
            sums = jnp.zeros((64, width), F32)
            for j in range(N):
                for buf in bufs:
                    v = f32(buf[j, half, rows, :])
                    sums = sums + v * v
            mean = jnp.sum(sums, axis=1, keepdims=True) * (1.0 / (N * 256))
            factor = lax.rsqrt(mean + EPS)
            for j in range(N):
                for k, buf in enumerate(bufs):
                    v = f32(buf[j, half, rows, :])
                    cols = pl.ds(j * 256 + k * width, width)
                    scale = f32(gain[cols].reshape(1, width))
                    out[pl.ds(half * 128 + part * 64, 64), cols] = (v * factor * scale).astype(BF)


def kernel(*refs):
    sources, refs = refs[:16], refs[16:]
    out, staged, in_sem, refs = refs[0], refs[1:17], refs[17], refs[18:]
    fetch = [
        pltpu.make_async_copy(source, target, in_sem.at[k])
        for k, (source, target) in enumerate(zip(sources, staged))
    ]
    for k in FIRST:
        fetch[k].start()
    for k in range(16):
        if k not in FIRST:
            fetch[k].start()
    body(fetch, out, *staged, *refs)


def body(
    fetch,
    out,
    tok,
    gain1,
    wb,
    wg,
    taps1,
    rmap,
    imap,
    rate,
    pld,
    wo,
    gain2,
    ug,
    uv,
    gtaps,
    vtaps,
    dn,
    gm,
    gu,
    gd,
    tokb,
    aftb,
    nrm,
    pair,
    mixed,
    gv,
    hid,
    part1,
    pair1,
    stage1,
    mid1,
    end1,
    part2,
    pair2,
    stage2,
    mid2,
    end2,
    ssem,
    rsem,
):
    z, y, t = lax.axis_index("fs_0"), lax.axis_index("fs_1"), lax.axis_index("tp")
    here = (z, y, t)
    wire = Wire(ssem, rsem)
    row = Row(z, y, t)
    mix = Spread(wire, "mix", 0, gm, CHUNKS[0], here)
    up = Spread(wire, "up", 1, gu, CHUNKS[1], here)
    down = Spread(wire, "dn", 2, gd, CHUNKS[2], here)
    ag1 = Gather(wire, "tok", tokb, row)
    ag2 = [Gather(wire, ("aft", k), aftb.at[k], row) for k in (0, 1)]
    rs1, rs2 = (
        [Sum(wire, (name, k), row, *(ref.at[k] for ref in refs)) for k in (0, 1)]
        for name, refs in (
            ("rs1", (part1, pair1, stage1, mid1, end1)),
            ("rs2", (part2, pair2, stage2, mid2, end2)),
        )
    )

    barrier = pltpu.get_barrier_semaphore()
    peers = [
        mix.neighbour(0, 1),
        mix.neighbour(0, -1),
        mix.neighbour(1, 1),
        mix.neighbour(1, -1),
        row.dev(row.right),
        row.dev(row.left),
        row.partner,
    ]
    for peer in peers:
        pl.semaphore_signal(barrier, inc=1, device_id=peer, device_id_type=MESH)

    split = (2, 16)
    for k in FIRST:
        fetch[k].wait()
    gm[z, y, :, :, 0:128] = wb[...].reshape(*split, 128)
    gm[z, y, :, :, 128:256] = wg[...].reshape(*split, 128)
    gm[z, y, :, :, 256:384] = wo[...].reshape(*split, 128)
    low, high = place(0), place(64)
    tokb[t] = tok[...].reshape(2, 128, 256)
    gu[z, y, :, :, 0:640] = ug[:, 0:640].reshape(*split, 640)
    gu[z, y, :, :, 640:1280] = uv[:, 0:640].reshape(*split, 640)
    tail = dot(ug[:, 640:704], low) + dot(uv[:, 640:704], high)
    gu[z, y, :, :, 1280:1408] = tail.astype(BF).reshape(*split, 128)
    gd[z, y, :, :, 0:640] = dn[:, 0:640].reshape(*split, 640)
    gd[z, y, :, :, 640:768] = dot(dn[:, 640:704], low).astype(BF).reshape(*split, 128)

    pl.semaphore_wait(barrier, len(peers))
    for k in range(16):
        if k not in FIRST:
            fetch[k].wait()

    pos = lax.broadcasted_iota(jnp.int32, (SEQ, 128), 0)
    lane = lax.broadcasted_iota(jnp.int32, (SEQ, 128), 1)

    def project():
        w = gm[:, :, :, :, 0:256].reshape(2048, 256)
        pair[...] = dot(nrm[...], w).astype(BF)

    def recurrence():
        rmat = jnp.concatenate([dot(rmap[0], low), dot(rmap[1], high)], axis=0).astype(BF)
        imat = jnp.concatenate([dot(imap[0], low), dot(imap[1], high)], axis=0).astype(BF)
        for s in range(4):
            rows = slice(s * SEQ, (s + 1) * SEQ)
            cv = conv(f32(pair[rows, 0:128]), f32(taps1[...]), pos).astype(BF)
            recur = jax.nn.sigmoid(dot(cv, rmat))
            inner = jax.nn.sigmoid(dot(cv, imat))
            loga = -DECAY_RATE_GAIN * recur * rate[...].reshape(1, 128) + pld[rows, :]
            a = jnp.exp(loga)
            d = jnp.sqrt(jnp.tanh(-loga) * (1.0 + a * a)) * inner * f32(cv)
            k = 1
            while k < SEQ:
                d = d + a * shifted(d, k, pos)
                if 2 * k < SEQ:
                    a = a * shifted(a, k, pos, 1.0)
                k *= 2
            mixed[rows, :] = (d * jax.nn.gelu(f32(pair[rows, 128:256]))).astype(BF)

    def mixer_out(k):
        for j in range(N):
            w = gm[j, 4 * k : 4 * k + 4, :, :, 256:384].reshape(128, 128)
            part1[k, j % 2, j // 2] = dot_t(mixed[...], w).astype(BF)

    def residual(k):
        cols = pl.ds(k * 128, 128)
        for half in (0, 1):
            rows = pl.ds(half * 128, 128)
            aftb[k, t, half] = (f32(tok[rows, cols]) + rs1[k].total(half)).astype(BF)

    def expand(k):
        cols = pl.ds(k * 256, 256 if k < 5 else 128)
        w = gu[:, :, :, :, cols]
        gv[:, cols] = dot(nrm[...], w.reshape(2048, w.shape[-1])).astype(BF)

    def gated():
        tail_taps = dot(gtaps[:, 640:704], low) + dot(vtaps[:, 640:704], high)
        for s in range(4):
            rows = pl.ds(s * SEQ, SEQ)
            for k in range(5):
                cols = pl.ds(k * 128, 128)
                g = conv(f32(gv[rows, cols]), f32(gtaps[:, cols]), pos)
                v = conv(f32(gv[rows, pl.ds(640 + k * 128, 128)]), f32(vtaps[:, cols]), pos)
                hid[rows, cols] = (jax.nn.silu(g) * v).astype(BF)
            b = conv(f32(gv[rows, pl.ds(1280, 128)]), tail_taps, pos)
            h = jnp.where(lane < 64, jax.nn.silu(b) * pltpu.roll(b, 64, 1), 0.0)
            hid[rows, pl.ds(640, 128)] = h.astype(BF)

    def contract():
        for j in range(N):
            sums = dot_t(hid[...], gd[j].reshape(256, 768)).astype(BF)
            for k in (0, 1):
                part2[k, j % 2, j // 2] = sums[:, k * 128 : k * 128 + 128]

    def result(k):
        cols = pl.ds(k * 128, 128)
        for half in (0, 1):
            rows = pl.ds(half * 128, 128)
            out[rows, cols] = (f32(aftb[k, t, half]) + rs2[k].total(half)).astype(BF)

    spreads = {"mix": mix, "up": up, "dn": down}
    steps = {
        ("norm1",): lambda: normed_into(nrm, (tokb,), gain1),
        ("win",): project,
        ("mixer",): recurrence,
        ("norm2",): lambda: normed_into(nrm, (aftb.at[0], aftb.at[1]), gain2),
        ("hid",): gated,
        ("part2",): contract,
    }
    for k in (0, 1):
        steps["part1", k] = functools.partial(mixer_out, k)
        steps["rs1", "total", k] = functools.partial(residual, k)
        steps["rs2", "total", k] = functools.partial(result, k)
    for name, k, gather in (("ag1", 0, ag1), ("ag2", 0, ag2[0]), ("ag2", 1, ag2[1])):
        steps[name, "start", k] = gather.start
        steps[name, "relay", k] = gather.relay
        steps[name, "share", k] = gather.share
        steps[name, "sharefar", k] = gather.share_far
        steps[name, "done", k] = gather.done
    for name, parts in (("rs1", rs1), ("rs2", rs2)):
        for k in (0, 1):
            steps[name, "start", k] = parts[k].start
            steps[name, "spread", k] = parts[k].spread
            steps[name, "relay", k] = parts[k].relay
    for step in ORDER:
        if step[0] in spreads:
            spread, what, rest = spreads[step[0]], step[1], step[2:]
            if what == "s1":
                spread.pass1(1)
            elif what == "f1":
                spread.forward1(*rest)
            elif what == "s2":
                spread.pass2(*rest, 1)
            else:
                spread.forward2(*rest)
        elif step[0] == "updot":
            expand(step[1])
        else:
            steps[step]()
    for part in (mix, up, down, ag1, *ag2, *rs1, *rs2):
        part.finish()


def per_device(*args):
    (tok, gain1, wb, wg, taps1, rmap, imap, rate, pld, wo, gain2, ug, uv, gtaps, vtaps, dn) = args
    sums = [
        pltpu.VMEM((2, 2, X, 256, 128), BF),
        pltpu.VMEM((2, X, 256, 128), BF),
        pltpu.VMEM((2, 6, 128, 128), BF),
        pltpu.VMEM((2, 2, 128, 128), BF),
        pltpu.VMEM((2, 2, 2, 128, 128), BF),
    ]
    operands = (
        tok, gain1, wb, wg, taps1, rmap, imap, rate, pld, wo.T, gain2, ug, uv, gtaps, vtaps, dn.T
    )
    return pl.pallas_call(
        kernel,
        out_shape=jax.ShapeDtypeStruct((256, 256), BF),
        in_specs=[pl.BlockSpec(memory_space=pltpu.HBM)] * 16,
        out_specs=pl.BlockSpec(memory_space=pltpu.VMEM),
        scratch_shapes=[
            *[pltpu.VMEM(a.shape, a.dtype) for a in operands],
            pltpu.SemaphoreType.DMA((16,)),
            pltpu.VMEM((N, N, 2, 16, 384), BF),
            pltpu.VMEM((N, N, 2, 16, 1408), BF),
            pltpu.VMEM((N, N, 2, 16, 768), BF),
            pltpu.VMEM((N, 2, 128, 256), BF),
            pltpu.VMEM((2, N, 2, 128, 128), BF),
            pltpu.VMEM((256, 2048), BF),
            pltpu.VMEM((256, 256), BF),
            pltpu.VMEM((256, 128), BF),
            pltpu.VMEM((256, 1408), BF),
            pltpu.VMEM((256, 768), BF),
            *sums,
            *sums,
            pltpu.SemaphoreType.DMA((SENDS,)),
            pltpu.SemaphoreType.DMA((ARRIVALS,)),
        ],
        compiler_params=pltpu.CompilerParams(
            collective_id=0, has_side_effects=True, vmem_limit_bytes=67043328
        ),
        name="layer",
    )(*operands)


def solution(mesh):
    torus = Mesh(mesh.devices.reshape(N, N, mesh.shape["tp"]), ("fs_0", "fs_1", "tp"))
    return jax.shard_map(
        per_device,
        mesh=torus,
        in_specs=(
            P(FS, "tp"),
            P(),
            P(FS, "tp"),
            P(FS, "tp"),
            P(None, "tp"),
            P("tp", None, None),
            P("tp", None, None),
            P("tp"),
            P(FS, "tp"),
            P("tp", FS),
            P(),
            P(FS, "tp"),
            P(FS, "tp"),
            P(None, "tp"),
            P(None, "tp"),
            P("tp", FS),
        ),
        out_specs=P(FS, "tp"),
        check_vma=False,
    )
```

time: 110 us -> 86.2 us (0.78)
  Pallas kernels: 100 us -> 84.3 us
  local copies, waits for them, and re-layouts: 9.17 us -> 1.57 us
    pallas_call x1, Pallas kernels: 100 us -> 84.3 us  [per_device(): pl.pallas_call(kernel, out_shape=jax.ShapeDtypeStruct((256, 256), BF), in...]
    unnamed x31 -> x1, local copies, waits for them, and re-layouts: 8.45 us -> 1.57 us
where the time goes in v2:
time: 86.2 us; the launch traced here: 85.9 us
  Pallas kernels  84.3 us (98%)
  local copies, waits for them, and re-layouts  1.57 us (2%)
    pallas_call x1, Pallas kernels, per_device(): pl.pallas_call(kernel, out_shape=jax.ShapeDtypeStruct((256, 256), BF), in...  84.3 us

profile of v2, /device:TPU:1, one launch (start us, length us, event | category | flops | bytes accessed | tf_op | source)
XLA Modules:
  0.0 85.9 jit_solution(12454177339899458920)
XLA Ops:
  0.0 84.3 %layer.1 = bf16[256,256]{1,0:T(8,128)(2,1)} custom-call(bf16[256,256]{1,0:T(8,128)(2,1)} %refs_0_.1, bf16[2048]{0:T(1024)(128)(2,1)} %refs_1_.1, bf16[32,128]{1,0:T(8,128)(2,1)} %refs_2_.1, bf16[32,128]{1,0:T(8,128)(2,1)} %refs_3_.1, bf16[4,128]{1,0:T(4,128)(2,1)} %refs_4_.1, bf16[2,64,64]{2,1,0:T(8,128)(2,1)} %refs_5_.1, bf16[2,64,64]{2,1,0:T(8,128)(2,1)} %refs_6_.1, ...), custom_call_target="tpu_custom_call" | custom-call | tf_op jit(solution)/shard_map/layer/pallas_call | solution.py:632
  84.3 1.6 %copy.18 = bf16[256,256]{1,0:T(8,128)(2,1)} copy(bf16[256,256]{1,0:T(8,128)(2,1)} %layer.1) | data formatting | bytes 262144

commit v3 on v2

--- a/solution.py
+++ b/solution.py
@@ -17,150 +17,178 @@
 MESH = pl.DeviceIdType.MESH
 N = 8
 X = 4
+MIX, UP, DN, AG1, AG2, RS1, RS2 = range(7)
+NORM1, WIN, MIXER, PART1, NORM2, UPDOT, HID, PART2 = range(7, 15)
+S1, F1, S2, F2, START, RELAY, SHARE, SHAREFAR, DONE, SPREAD, REST, TOTAL = range(12)
 SENDS = 14
-ARRIVALS = 100
-CHUNKS = (4, 8, 4)
+ARRIVALS = 120
+CHUNKS = (4, 8, 8)
 ORDER = (
-    ("mix", "s1"),
-    ("ag1", "start", 0),
-    ("up", "s1"),
-    ("up", "s2", 0),
-    ("dn", "s1"),
-    ("mix", "f1", 1),
-    ("mix", "s2", 0),
-    ("up", "f1", 1),
-    ("up", "s2", 7),
-    ("dn", "f1", 1),
-    ("mix", "f1", 2),
-    ("up", "s2", 1),
-    ("up", "f2", 0, 1),
-    ("up", "f1", 2),
-    ("mix", "f2", 0, 1),
-    ("ag1", "relay", 0),
-    ("mix", "f1", 3),
-    ("mix", "s2", 1),
-    ("up", "s2", 2),
-    ("mix", "s2", 3),
-    ("dn", "f1", 2),
-    ("up", "f2", 7, 1),
-    ("mix", "f1", 4),
-    ("mix", "s2", 2),
-    ("mix", "f2", 1, 1),
-    ("up", "f1", 3),
-    ("dn", "s2", 0),
-    ("mix", "f2", 3, 1),
-    ("ag1", "share", 0),
-    ("up", "f2", 2, 1),
-    ("ag1", "sharefar", 0),
-    ("mix", "f2", 2, 1),
-    ("mix", "f2", 0, 2),
-    ("up", "f2", 1, 1),
-    ("mix", "f2", 1, 2),
-    ("up", "s2", 3),
-    ("up", "f2", 0, 2),
-    ("mix", "f2", 2, 2),
-    ("up", "f1", 4),
-    ("mix", "f2", 3, 2),
-    ("ag1", "done", 0),
-    ("up", "s2", 4),
-    ("dn", "f1", 3),
-    ("up", "s2", 5),
-    ("mix", "f2", 1, 3),
-    ("norm1",),
-    ("up", "s2", 6),
-    ("mix", "f2", 0, 3),
-    ("mix", "f2", 2, 3),
-    ("mix", "f2", 3, 3),
-    ("up", "f2", 4, 1),
-    ("dn", "f1", 4),
-    ("dn", "s2", 3),
-    ("up", "f2", 3, 1),
-    ("up", "f2", 1, 2),
-    ("up", "f2", 5, 1),
-    ("mix", "f2", 0, 4),
-    ("mix", "f2", 3, 4),
-    ("up", "f2", 7, 2),
-    ("mix", "f2", 1, 4),
-    ("up", "f2", 2, 2),
-    ("up", "f2", 0, 3),
-    ("mix", "f2", 2, 4),
-    ("win",),
-    ("mixer",),
-    ("part1", 0),
-    ("rs1", "start", 0),
-    ("up", "f2", 6, 1),
-    ("part1", 1),
-    ("rs1", "start", 1),
-    ("dn", "s2", 1),
-    ("rs1", "spread", 0),
-    ("up", "f2", 3, 2),
-    ("dn", "s2", 2),
-    ("up", "f2", 4, 2),
-    ("rs1", "spread", 1),
-    ("rs1", "relay", 0),
-    ("up", "f2", 5, 2),
-    ("rs1", "relay", 1),
-    ("up", "f2", 6, 2),
-    ("up", "f2", 7, 3),
-    ("dn", "f2", 1, 1),
-    ("rs1", "total", 0),
-    ("up", "f2", 1, 3),
-    ("ag2", "start", 0),
-    ("up", "f2", 3, 3),
-    ("dn", "f2", 0, 1),
-    ("rs1", "total", 1),
-    ("ag2", "start", 1),
-    ("up", "f2", 4, 3),
-    ("up", "f2", 5, 3),
-    ("up", "f2", 6, 3),
-    ("dn", "f2", 3, 1),
-    ("up", "f2", 2, 3),
-    ("dn", "f2", 2, 1),
-    ("ag2", "relay", 0),
-    ("ag2", "relay", 1),
-    ("ag2", "share", 1),
-    ("ag2", "share", 0),
-    ("dn", "f2", 0, 2),
-    ("up", "f2", 5, 4),
-    ("ag2", "sharefar", 0),
-    ("dn", "f2", 1, 2),
-    ("dn", "f2", 3, 2),
-    ("up", "f2", 1, 4),
-    ("ag2", "sharefar", 1),
-    ("up", "f2", 4, 4),
-    ("up", "f2", 7, 4),
-    ("up", "f2", 3, 4),
-    ("up", "f2", 6, 4),
-    ("up", "f2", 2, 4),
-    ("dn", "f2", 2, 2),
-    ("ag2", "done", 0),
-    ("dn", "f2", 0, 3),
-    ("ag2", "done", 1),
-    ("norm2",),
-    ("up", "f2", 0, 4),
-    ("updot", 1),
-    ("dn", "f2", 1, 3),
-    ("updot", 3),
-    ("dn", "f2", 3, 3),
-    ("updot", 0),
-    ("dn", "f2", 2, 3),
-    ("updot", 5),
-    ("updot", 2),
-    ("updot", 4),
-    ("dn", "f2", 1, 4),
-    ("dn", "f2", 0, 4),
-    ("hid",),
-    ("dn", "f2", 3, 4),
-    ("dn", "f2", 2, 4),
-    ("part2",),
-    ("rs2", "start", 0),
-    ("rs2", "start", 1),
-    ("rs2", "spread", 0),
-    ("rs2", "spread", 1),
-    ("rs2", "relay", 0),
-    ("rs2", "relay", 1),
-    ("rs2", "total", 0),
-    ("rs2", "total", 1),
+    (MIX, S1),
+    (DN, S1),
+    (UP, S1),
+    (DN, S2, 0),
+    (UP, S2, 0),
+    (MIX, F1, 1),
+    (MIX, S2, 0),
+    (DN, F1, 1),
+    (DN, S2, 7),
+    (UP, F1, 1),
+    (DN, S2, 1),
+    (UP, S2, 1),
+    (AG1, START, 0),
+    (MIX, F1, 2),
+    (UP, S2, 7),
+    (UP, F2, 0, 1),
+    (MIX, F2, 0, 1),
+    (UP, F1, 2),
+    (MIX, F1, 3),
+    (AG1, RELAY, 0),
+    (AG1, SHARE, 0),
+    (MIX, S2, 3),
+    (MIX, S2, 1),
+    (UP, S2, 2),
+    (UP, F2, 1, 1),
+    (DN, F1, 2),
+    (MIX, F1, 4),
+    (MIX, S2, 2),
+    (UP, F1, 3),
+    (MIX, F2, 1, 1),
+    (AG1, SHAREFAR, 0),
+    (MIX, F2, 3, 1),
+    (UP, F2, 7, 1),
+    (DN, S2, 2),
+    (AG1, DONE, 0),
+    (MIX, F2, 0, 2),
+    (MIX, F2, 2, 1),
+    (UP, S2, 5),
+    (UP, F1, 4),
+    (MIX, F2, 1, 2),
+    (MIX, F2, 3, 2),
+    (UP, S2, 4),
+    (MIX, F2, 0, 3),
+    (MIX, F2, 2, 2),
+    (UP, S2, 3),
+    (UP, F2, 5, 1),
+    (MIX, F2, 1, 3),
+    (UP, F2, 2, 1),
+    (MIX, F2, 3, 3),
+    (DN, F1, 3),
+    (MIX, F2, 2, 3),
+    (DN, S2, 5),
+    (DN, S2, 6),
+    (UP, S2, 6),
+    (UP, F2, 3, 1),
+    (UP, F2, 4, 1),
+    (UP, F2, 1, 2),
+    (DN, F2, 7, 1),
+    (NORM1,),
+    (MIX, F2, 1, 4),
+    (UP, F2, 7, 2),
+    (MIX, F2, 0, 4),
+    (DN, S2, 3),
+    (MIX, F2, 3, 4),
+    (MIX, F2, 2, 4),
+    (WIN,),
+    (MIXER,),
+    (PART1, 1),
+    (RS1, START, 1),
+    (PART1, 0),
+    (RS1, START, 0),
+    (RS1, SPREAD, 1),
+    (UP, F2, 6, 1),
+    (UP, F2, 5, 2),
+    (RS1, SPREAD, 0),
+    (UP, F2, 2, 2),
+    (RS1, REST, 1),
+    (DN, F1, 4),
+    (RS1, REST, 0),
+    (DN, F2, 5, 1),
+    (UP, F2, 3, 2),
+    (DN, F2, 2, 1),
+    (RS1, RELAY, 1),
+    (DN, F2, 3, 1),
+    (UP, F2, 0, 2),
+    (DN, S2, 4),
+    (RS1, RELAY, 0),
+    (UP, F2, 4, 2),
+    (UP, F2, 6, 2),
+    (RS1, TOTAL, 1),
+    (AG2, START, 1),
+    (UP, F2, 1, 3),
+    (DN, F2, 6, 1),
+    (UP, F2, 7, 3),
+    (DN, F2, 0, 1),
+    (DN, F2, 1, 1),
+    (RS1, TOTAL, 0),
+    (AG2, START, 0),
+    (UP, F2, 5, 3),
+    (AG2, RELAY, 1),
+    (UP, F2, 3, 3),
+    (UP, F2, 2, 3),
+    (UP, F2, 6, 3),
+    (UP, F2, 0, 3),
+    (AG2, SHARE, 1),
+    (AG2, RELAY, 0),
+    (UP, F2, 4, 3),
+    (DN, F2, 4, 1),
+    (DN, F2, 7, 2),
+    (DN, F2, 2, 2),
+    (DN, F2, 1, 2),
+    (UP, F2, 7, 4),
+    (AG2, SHAREFAR, 1),
+    (DN, F2, 6, 2),
+    (AG2, SHARE, 0),
+    (DN, F2, 3, 2),
+    (DN, F2, 0, 2),
+    (DN, F2, 5, 2),
+    (AG2, SHAREFAR, 0),
+    (UP, F2, 1, 4),
+    (UP, F2, 6, 4),
+    (AG2, DONE, 1),
+    (UP, F2, 0, 4),
+    (UP, F2, 2, 4),
+    (DN, F2, 4, 2),
+    (UP, F2, 3, 4),
+    (UP, F2, 5, 4),
+    (UP, F2, 4, 4),
+    (AG2, DONE, 0),
+    (NORM2,),
+    (UPDOT, 0),
+    (DN, F2, 2, 3),
+    (DN, F2, 7, 3),
+    (UPDOT, 4),
+    (DN, F2, 1, 3),
+    (DN, F2, 6, 3),
+    (DN, F2, 3, 3),
+    (UPDOT, 5),
+    (DN, F2, 0, 3),
+    (DN, F2, 5, 3),
+    (UPDOT, 2),
+    (DN, F2, 4, 3),
+    (UPDOT, 1),
+    (UPDOT, 3),
+    (DN, F2, 2, 4),
+    (HID,),
+    (DN, F2, 1, 4),
+    (DN, F2, 7, 4),
+    (DN, F2, 6, 4),
+    (DN, F2, 0, 4),
+    (DN, F2, 3, 4),
+    (DN, F2, 5, 4),
+    (PART2, 0),
+    (DN, F2, 4, 4),
+    (PART2, 1),
+    (RS2, START, 0),
+    (RS2, START, 1),
+    (RS2, SPREAD, 0),
+    (RS2, SPREAD, 1),
+    (RS2, REST, 0),
+    (RS2, REST, 1),
+    (RS2, RELAY, 0),
+    (RS2, RELAY, 1),
+    (RS2, TOTAL, 0),
+    (RS2, TOTAL, 1),
 )
 FIRST = (2, 3, 9, 0, 11, 12, 15)
 
@@ -343,7 +371,9 @@
 
     def start(self):
         r = self.row
-        self.wire.go(self.key(0), self.key(0), self.part.at[1 - r.c], self.pair, r.partner)
+        for x, key in ((r.across, 0), (r.right, 3), (r.left, 3), (r.x, 3)):
+            src, dst = self.part.at[1 - r.c, x], self.pair.at[x]
+            self.wire.go(self.key(0), self.key(key), src, dst, r.partner)
 
     def both(self, x, half):
         rows = pl.ds(half * 128, 128)
@@ -357,9 +387,13 @@
 
     def spread(self):
         r = self.row
-        self.wire.got(self.key(0), self.pair)
+        self.wire.got(self.key(0), self.pair.at[0])
         self.out(0, self.both(r.across, 0), self.mid.at[0], 1)
         self.out(1, self.both(r.across, 1), self.mid.at[1], -1)
+
+    def rest(self):
+        r = self.row
+        self.wire.got(self.key(3), self.pair.at[pl.ds(0, 3)])
         self.out(2, self.both(r.right, 1), self.end.at[0, 1], 1)
         self.out(3, self.both(r.left, 0), self.end.at[1, 0], -1)
 
@@ -412,11 +446,12 @@
     for k in range(16):
         if k not in FIRST:
             fetch[k].start()
-    body(fetch, out, *staged, *refs)
+    body(fetch, in_sem, out, *staged, *refs)
 
 
 def body(
     fetch,
+    in_sem,
     out,
     tok,
     gain1,
@@ -454,6 +489,7 @@
     stage2,
     mid2,
     end2,
+    final,
     ssem,
     rsem,
 ):
@@ -488,24 +524,31 @@
         pl.semaphore_signal(barrier, inc=1, device_id=peer, device_id_type=MESH)
 
     split = (2, 16)
-    for k in FIRST:
-        fetch[k].wait()
+    low, high = place(0), place(64)
+
+    def ready(*which):
+        for k in which:
+            fetch[k].wait()
+
+    def prepare():
+        ready(0, 11, 12, 15)
+        tokb[t] = tok[...].reshape(2, 128, 256)
+        gu[z, y, :, :, 0:640] = ug[:, 0:640].reshape(*split, 640)
+        gu[z, y, :, :, 640:1280] = uv[:, 0:640].reshape(*split, 640)
+        tail = dot(ug[:, 640:704], low) + dot(uv[:, 640:704], high)
+        gu[z, y, :, :, 1280:1408] = tail.astype(BF).reshape(*split, 128)
+        gd[z, y, :, :, 0:640] = dn[:, 0:640].reshape(*split, 640)
+        gd[z, y, :, :, 640:768] = dot(dn[:, 640:704], low).astype(BF).reshape(*split, 128)
+
+    def start_norm():
+        ready(*(k for k in range(16) if k not in FIRST))
+        normed_into(nrm, (tokb,), gain1)
+
+    ready(2, 3, 9)
     gm[z, y, :, :, 0:128] = wb[...].reshape(*split, 128)
     gm[z, y, :, :, 128:256] = wg[...].reshape(*split, 128)
     gm[z, y, :, :, 256:384] = wo[...].reshape(*split, 128)
-    low, high = place(0), place(64)
-    tokb[t] = tok[...].reshape(2, 128, 256)
-    gu[z, y, :, :, 0:640] = ug[:, 0:640].reshape(*split, 640)
-    gu[z, y, :, :, 640:1280] = uv[:, 0:640].reshape(*split, 640)
-    tail = dot(ug[:, 640:704], low) + dot(uv[:, 640:704], high)
-    gu[z, y, :, :, 1280:1408] = tail.astype(BF).reshape(*split, 128)
-    gd[z, y, :, :, 0:640] = dn[:, 0:640].reshape(*split, 640)
-    gd[z, y, :, :, 640:768] = dot(dn[:, 640:704], low).astype(BF).reshape(*split, 128)
-
     pl.semaphore_wait(barrier, len(peers))
-    for k in range(16):
-        if k not in FIRST:
-            fetch[k].wait()
 
     pos = lax.broadcasted_iota(jnp.int32, (SEQ, 128), 0)
     lane = lax.broadcasted_iota(jnp.int32, (SEQ, 128), 1)
@@ -562,59 +605,70 @@
             h = jnp.where(lane < 64, jax.nn.silu(b) * pltpu.roll(b, 64, 1), 0.0)
             hid[rows, pl.ds(640, 128)] = h.astype(BF)
 
-    def contract():
-        for j in range(N):
+    def contract(late):
+        for q in (N // 2,) if late else [q for q in range(N) if q != N // 2]:
+            j = lax.rem(z + q, N)
             sums = dot_t(hid[...], gd[j].reshape(256, 768)).astype(BF)
             for k in (0, 1):
-                part2[k, j % 2, j // 2] = sums[:, k * 128 : k * 128 + 128]
+                part2[k, lax.rem(j, 2), j // 2] = sums[:, k * 128 : k * 128 + 128]
 
     def result(k):
         cols = pl.ds(k * 128, 128)
         for half in (0, 1):
             rows = pl.ds(half * 128, 128)
-            out[rows, cols] = (f32(aftb[k, t, half]) + rs2[k].total(half)).astype(BF)
-
-    spreads = {"mix": mix, "up": up, "dn": down}
+            final[k, rows, :] = (f32(aftb[k, t, half]) + rs2[k].total(half)).astype(BF)
+        pltpu.make_async_copy(final.at[k], out.at[:, cols], in_sem.at[k]).start()
+
+    spreads = {MIX: mix, UP: up, DN: down}
     steps = {
-        ("norm1",): lambda: normed_into(nrm, (tokb,), gain1),
-        ("win",): project,
-        ("mixer",): recurrence,
-        ("norm2",): lambda: normed_into(nrm, (aftb.at[0], aftb.at[1]), gain2),
-        ("hid",): gated,
-        ("part2",): contract,
+        (NORM1,): start_norm,
+        (WIN,): project,
+        (MIXER,): recurrence,
+        (NORM2,): lambda: normed_into(nrm, (aftb.at[0], aftb.at[1]), gain2),
+        (HID,): gated,
+        (PART2, 0): lambda: contract(False),
+        (PART2, 1): lambda: contract(True),
     }
+    for k in range(6):
+        steps[UPDOT, k] = functools.partial(expand, k)
     for k in (0, 1):
-        steps["part1", k] = functools.partial(mixer_out, k)
-        steps["rs1", "total", k] = functools.partial(residual, k)
-        steps["rs2", "total", k] = functools.partial(result, k)
-    for name, k, gather in (("ag1", 0, ag1), ("ag2", 0, ag2[0]), ("ag2", 1, ag2[1])):
-        steps[name, "start", k] = gather.start
-        steps[name, "relay", k] = gather.relay
-        steps[name, "share", k] = gather.share
-        steps[name, "sharefar", k] = gather.share_far
-        steps[name, "done", k] = gather.done
-    for name, parts in (("rs1", rs1), ("rs2", rs2)):
+        steps[PART1, k] = functools.partial(mixer_out, k)
+        steps[RS1, TOTAL, k] = functools.partial(residual, k)
+        steps[RS2, TOTAL, k] = functools.partial(result, k)
+    for name, k, gather in ((AG1, 0, ag1), (AG2, 0, ag2[0]), (AG2, 1, ag2[1])):
+        steps[name, START, k] = gather.start
+        steps[name, RELAY, k] = gather.relay
+        steps[name, SHARE, k] = gather.share
+        steps[name, SHAREFAR, k] = gather.share_far
+        steps[name, DONE, k] = gather.done
+    for name, parts in ((RS1, rs1), (RS2, rs2)):
         for k in (0, 1):
-            steps[name, "start", k] = parts[k].start
-            steps[name, "spread", k] = parts[k].spread
-            steps[name, "relay", k] = parts[k].relay
+            steps[name, START, k] = parts[k].start
+            steps[name, SPREAD, k] = parts[k].spread
+            steps[name, REST, k] = parts[k].rest
+            steps[name, RELAY, k] = parts[k].relay
+    prepared = False
     for step in ORDER:
-        if step[0] in spreads:
-            spread, what, rest = spreads[step[0]], step[1], step[2:]
-            if what == "s1":
-                spread.pass1(1)
-            elif what == "f1":
-                spread.forward1(*rest)
-            elif what == "s2":
-                spread.pass2(*rest, 1)
-            else:
-                spread.forward2(*rest)
-        elif step[0] == "updot":
-            expand(step[1])
+        if not prepared and step[0] != MIX:
+            prepare()
+            prepared = True
+        if step[0] not in spreads:
+            steps[step]()
+            continue
+        spread, what, rest = spreads[step[0]], step[1], step[2:]
+        if what == S1:
+            spread.pass1(1)
+        elif what == F1:
+            spread.forward1(*rest)
+        elif what == S2:
+            spread.pass2(*rest, 1)
         else:
-            steps[step]()
+            spread.forward2(*rest)
     for part in (mix, up, down, ag1, *ag2, *rs1, *rs2):
         part.finish()
+    for k in (0, 1):
+        cols = pl.ds(k * 128, 128)
+        pltpu.make_async_copy(final.at[k], out.at[:, cols], in_sem.at[k]).wait()
 
 
 def per_device(*args):
@@ -633,7 +687,7 @@
         kernel,
         out_shape=jax.ShapeDtypeStruct((256, 256), BF),
         in_specs=[pl.BlockSpec(memory_space=pltpu.HBM)] * 16,
-        out_specs=pl.BlockSpec(memory_space=pltpu.VMEM),
+        out_specs=pl.BlockSpec(memory_space=pltpu.HBM),
         scratch_shapes=[
             *[pltpu.VMEM(a.shape, a.dtype) for a in operands],
             pltpu.SemaphoreType.DMA((16,)),
@@ -649,6 +703,7 @@
             pltpu.VMEM((256, 768), BF),
             *sums,
             *sums,
+            pltpu.VMEM((2, 256, 128), BF),
             pltpu.SemaphoreType.DMA((SENDS,)),
             pltpu.SemaphoreType.DMA((ARRIVALS,)),
         ],

time: 86.2 us -> 85.2 us (0.988)
  no operation moved by 1% of the time
where the time goes in v3:
time: 85.2 us; the launch traced here: 85.1 us
  Pallas kernels  83.5 us (98%)
  local copies, waits for them, and re-layouts  1.57 us (2%)
    pallas_call x1, Pallas kernels, per_device(): pl.pallas_call(kernel, out_shape=jax.ShapeDtypeStruct((256, 256), BF), in...  83.5 us

profile of v3, /device:TPU:1, one launch (start us, length us, event | category | flops | bytes accessed | tf_op | source)
XLA Modules:
  0.0 85.1 jit_solution(1827619301387233939)
XLA Ops:
  0.0 83.5 %layer.1 = bf16[256,256]{1,0:T(8,128)(2,1)} custom-call(bf16[256,256]{1,0:T(8,128)(2,1)} %refs_0_.1, bf16[2048]{0:T(1024)(128)(2,1)} %refs_1_.1, bf16[32,128]{1,0:T(8,128)(2,1)} %refs_2_.1, bf16[32,128]{1,0:T(8,128)(2,1)} %refs_3_.1, bf16[4,128]{1,0:T(4,128)(2,1)} %refs_4_.1, bf16[2,64,64]{2,1,0:T(8,128)(2,1)} %refs_5_.1, bf16[2,64,64]{2,1,0:T(8,128)(2,1)} %refs_6_.1, ...), custom_call_target="tpu_custom_call" | custom-call | tf_op jit(solution)/shard_map/layer/pallas_call | solution.py:686
  83.5 1.6 %copy.18 = bf16[256,256]{1,0:T(8,128)(2,1)} copy(bf16[256,256]{1,0:T(8,128)(2,1)} %layer.1) | data formatting | bytes 262144

commit v4 on v3

--- a/solution.py
+++ b/solution.py
@@ -32,62 +32,64 @@
     (MIX, F1, 1),
     (MIX, S2, 0),
     (DN, F1, 1),
-    (DN, S2, 7),
+    (DN, S2, 1),
     (UP, F1, 1),
-    (DN, S2, 1),
+    (DN, F2, 0, 1),
+    (AG1, START, 0),
     (UP, S2, 1),
-    (AG1, START, 0),
     (MIX, F1, 2),
     (UP, S2, 7),
     (UP, F2, 0, 1),
     (MIX, F2, 0, 1),
     (UP, F1, 2),
     (MIX, F1, 3),
+    (DN, F1, 2),
+    (MIX, S2, 1),
     (AG1, RELAY, 0),
-    (AG1, SHARE, 0),
     (MIX, S2, 3),
-    (MIX, S2, 1),
+    (UP, F2, 1, 1),
     (UP, S2, 2),
-    (UP, F2, 1, 1),
-    (DN, F1, 2),
+    (MIX, F2, 0, 2),
     (MIX, F1, 4),
     (MIX, S2, 2),
+    (MIX, F2, 1, 1),
+    (MIX, F2, 3, 1),
+    (DN, F1, 3),
+    (UP, F2, 7, 1),
+    (DN, S2, 6),
     (UP, F1, 3),
-    (MIX, F2, 1, 1),
+    (MIX, F2, 2, 1),
+    (AG1, SHARE, 0),
     (AG1, SHAREFAR, 0),
-    (MIX, F2, 3, 1),
-    (UP, F2, 7, 1),
-    (DN, S2, 2),
-    (AG1, DONE, 0),
-    (MIX, F2, 0, 2),
-    (MIX, F2, 2, 1),
-    (UP, S2, 5),
-    (UP, F1, 4),
+    (MIX, F2, 0, 3),
+    (DN, F2, 1, 1),
     (MIX, F2, 1, 2),
     (MIX, F2, 3, 2),
+    (UP, S2, 5),
+    (DN, S2, 7),
+    (UP, F1, 4),
+    (MIX, F2, 2, 2),
+    (UP, F2, 2, 1),
+    (UP, S2, 3),
+    (MIX, F2, 1, 3),
+    (MIX, F2, 3, 3),
+    (MIX, F2, 0, 4),
     (UP, S2, 4),
-    (MIX, F2, 0, 3),
-    (MIX, F2, 2, 2),
-    (UP, S2, 3),
+    (DN, F1, 4),
+    (AG1, DONE, 0),
+    (MIX, F2, 2, 3),
+    (UP, S2, 6),
+    (NORM1,),
+    (DN, F2, 7, 1),
     (UP, F2, 5, 1),
-    (MIX, F2, 1, 3),
-    (UP, F2, 2, 1),
-    (MIX, F2, 3, 3),
-    (DN, F1, 3),
-    (MIX, F2, 2, 3),
-    (DN, S2, 5),
-    (DN, S2, 6),
-    (UP, S2, 6),
     (UP, F2, 3, 1),
+    (UP, F2, 7, 2),
+    (DN, S2, 2),
+    (MIX, F2, 1, 4),
+    (DN, S2, 4),
     (UP, F2, 4, 1),
+    (MIX, F2, 3, 4),
     (UP, F2, 1, 2),
-    (DN, F2, 7, 1),
-    (NORM1,),
-    (MIX, F2, 1, 4),
-    (UP, F2, 7, 2),
-    (MIX, F2, 0, 4),
-    (DN, S2, 3),
-    (MIX, F2, 3, 4),
     (MIX, F2, 2, 4),
     (WIN,),
     (MIXER,),
@@ -96,85 +98,83 @@
     (PART1, 0),
     (RS1, START, 0),
     (RS1, SPREAD, 1),
+    (DN, S2, 5),
     (UP, F2, 6, 1),
+    (RS1, SPREAD, 0),
+    (UP, F2, 0, 2),
+    (DN, S2, 3),
+    (UP, F2, 3, 2),
+    (RS1, REST, 0),
+    (RS1, REST, 1),
     (UP, F2, 5, 2),
-    (RS1, SPREAD, 0),
+    (RS1, RELAY, 1),
+    (UP, F2, 4, 2),
+    (RS1, RELAY, 0),
     (UP, F2, 2, 2),
-    (RS1, REST, 1),
-    (DN, F1, 4),
-    (RS1, REST, 0),
-    (DN, F2, 5, 1),
-    (UP, F2, 3, 2),
-    (DN, F2, 2, 1),
-    (RS1, RELAY, 1),
-    (DN, F2, 3, 1),
-    (UP, F2, 0, 2),
-    (DN, S2, 4),
-    (RS1, RELAY, 0),
-    (UP, F2, 4, 2),
     (UP, F2, 6, 2),
     (RS1, TOTAL, 1),
     (AG2, START, 1),
+    (DN, F2, 2, 1),
+    (DN, F2, 6, 1),
+    (UP, F2, 3, 3),
+    (DN, F2, 3, 1),
     (UP, F2, 1, 3),
-    (DN, F2, 6, 1),
-    (UP, F2, 7, 3),
-    (DN, F2, 0, 1),
-    (DN, F2, 1, 1),
+    (DN, F2, 5, 1),
     (RS1, TOTAL, 0),
     (AG2, START, 0),
-    (UP, F2, 5, 3),
+    (UP, F2, 0, 3),
+    (UP, F2, 2, 3),
     (AG2, RELAY, 1),
-    (UP, F2, 3, 3),
-    (UP, F2, 2, 3),
     (UP, F2, 6, 3),
-    (UP, F2, 0, 3),
-    (AG2, SHARE, 1),
+    (UP, F2, 7, 3),
     (AG2, RELAY, 0),
     (UP, F2, 4, 3),
+    (UP, F2, 5, 3),
     (DN, F2, 4, 1),
+    (DN, F2, 1, 2),
+    (AG2, SHARE, 0),
+    (DN, F2, 6, 2),
+    (DN, F2, 0, 2),
     (DN, F2, 7, 2),
+    (AG2, SHARE, 1),
+    (UP, F2, 3, 4),
     (DN, F2, 2, 2),
-    (DN, F2, 1, 2),
-    (UP, F2, 7, 4),
+    (UP, F2, 1, 4),
+    (DN, F2, 3, 2),
     (AG2, SHAREFAR, 1),
-    (DN, F2, 6, 2),
-    (AG2, SHARE, 0),
-    (DN, F2, 3, 2),
-    (DN, F2, 0, 2),
     (DN, F2, 5, 2),
     (AG2, SHAREFAR, 0),
-    (UP, F2, 1, 4),
-    (UP, F2, 6, 4),
     (AG2, DONE, 1),
     (UP, F2, 0, 4),
     (UP, F2, 2, 4),
+    (UP, F2, 5, 4),
+    (UP, F2, 6, 4),
+    (UP, F2, 4, 4),
+    (UP, F2, 7, 4),
     (DN, F2, 4, 2),
-    (UP, F2, 3, 4),
-    (UP, F2, 5, 4),
-    (UP, F2, 4, 4),
     (AG2, DONE, 0),
     (NORM2,),
-    (UPDOT, 0),
-    (DN, F2, 2, 3),
-    (DN, F2, 7, 3),
-    (UPDOT, 4),
+    (UPDOT, 5),
     (DN, F2, 1, 3),
     (DN, F2, 6, 3),
+    (UPDOT, 4),
+    (DN, F2, 0, 3),
+    (DN, F2, 7, 3),
+    (DN, F2, 2, 3),
+    (UPDOT, 0),
     (DN, F2, 3, 3),
-    (UPDOT, 5),
-    (DN, F2, 0, 3),
     (DN, F2, 5, 3),
+    (UPDOT, 1),
+    (DN, F2, 4, 3),
     (UPDOT, 2),
-    (DN, F2, 4, 3),
-    (UPDOT, 1),
     (UPDOT, 3),
-    (DN, F2, 2, 4),
     (HID,),
+    (DN, F2, 6, 4),
     (DN, F2, 1, 4),
-    (DN, F2, 7, 4),
-    (DN, F2, 6, 4),
     (DN, F2, 0, 4),
     (DN, F2, 3, 4),
+    (DN, F2, 2, 4),
+    (DN, F2, 7, 4),
     (DN, F2, 5, 4),
     (PART2, 0),
     (DN, F2, 4, 4),

time: 85.2 us -> 85.8 us (level)
  no operation moved by 1% of the time
where the time goes in v4:
time: 85.8 us; the launch traced here: 85.7 us
  Pallas kernels  84.1 us (98%)
  local copies, waits for them, and re-layouts  1.57 us (2%)
    pallas_call x1, Pallas kernels, per_device(): pl.pallas_call(kernel, out_shape=jax.ShapeDtypeStruct((256, 256), BF), in...  84.1 us

profile of v4, /device:TPU:1, one launch (start us, length us, event | category | flops | bytes accessed | tf_op | source)
XLA Modules:
  0.0 85.7 jit_solution(424127565082558131)
XLA Ops:
  0.0 84.1 %layer.1 = bf16[256,256]{1,0:T(8,128)(2,1)} custom-call(bf16[256,256]{1,0:T(8,128)(2,1)} %refs_0_.1, bf16[2048]{0:T(1024)(128)(2,1)} %refs_1_.1, bf16[32,128]{1,0:T(8,128)(2,1)} %refs_2_.1, bf16[32,128]{1,0:T(8,128)(2,1)} %refs_3_.1, bf16[4,128]{1,0:T(4,128)(2,1)} %refs_4_.1, bf16[2,64,64]{2,1,0:T(8,128)(2,1)} %refs_5_.1, bf16[2,64,64]{2,1,0:T(8,128)(2,1)} %refs_6_.1, ...), custom_call_target="tpu_custom_call" | custom-call | tf_op jit(solution)/shard_map/layer/pallas_call | solution.py:686
  84.1 1.6 %copy.18 = bf16[256,256]{1,0:T(8,128)(2,1)} copy(bf16[256,256]{1,0:T(8,128)(2,1)} %layer.1) | data formatting | bytes 262144
